TPU v7x, 256 devices: a whole 4x4x8 slice. The times are simulated.
256 devices in a mesh: sp: 32 (over z, y), tp: 8 (over x, core).
Axes of the slice: x: 4, y: 4, z: 8, core: 2. Of those that a mesh axis runs over, the one named last changes fastest.
Arguments:
- mix_input: bfloat16 [8192, 1024], P('sp', 'tp'), may hold values from -6 to 6
- stream: bfloat16 [8192, 2048], P(('sp', 'tp')), may hold values from -48 to 48
- doc_ids: int32 [8192], P('sp'), may hold values from 0 to 3, never falling along the last dimension, each value on 1 to 4096 neighbouring positions
- log_dt: float32 [64], P('tp'), may hold values from -12 to -2
- decay_rate: float32 [64, 64], P('tp'), may hold values from 0.5 to 1
- frequency: float32 [64, 64], P('tp'), may hold values from 0 to 64
- input_real: float32 [2, 64, 64, 16], P(None, 'tp'), may hold values from -400 to 400
- input_imag: float32 [2, 64, 64, 16], P(None, 'tp'), may hold values from -400 to 400
- output_real: float32 [2, 64, 16, 64], P(None, 'tp'), may hold values from -0.75 to 0.75
- output_imag: float32 [2, 64, 16, 64], P(None, 'tp'), may hold values from -0.75 to 0.75
- skip_gain: float32 [1024], P('tp'), may hold values from -4 to 4
- log_keep: float32 [64, 8192], P('tp', 'sp'), may hold values from -2 to 0
- proj_weight: bfloat16 [1024, 2048], P('tp'), may hold values from -0.1875 to 0.1875
- norm_gain: float32 [2048], replicated, may hold values from 0.1 to 1.9
- gate_weight: bfloat16 [2048, 5632], P('sp', 'tp'), may hold values from -0.125 to 0.125
- up_weight: bfloat16 [2048, 5632], P('sp', 'tp'), may hold values from -0.125 to 0.125
- down_weight: bfloat16 [5632, 2048], P('tp', 'sp'), may hold values from -0.078125 to 0.078125
Outputs:
- layer_out: bfloat16 [8192, 2048], P(('sp', 'tp'))
Inputs may be any that keep to these rules, and one draw needn't show every extreme that they name: `doc_ids`: document numbers never fall along the positions; a document covers at most half of the positions.
All inputs are finite; a program needn't handle non-finite values.
Results may differ from a plain program's by a relative error of at most 0.009.
Values may be sent and summed in bfloat16 or wider, within the bound.
No kernel may reach another device: no remote copies, remote signals or barrier semaphores. Data moves between devices by JAX's collectives and lax.ppermute only.
A program may use at most 128 MiB of HBM per device.

v0:
```python
import jax
import jax.numpy as jnp
from jax import lax
from jax.sharding import Mesh
from jax.sharding import PartitionSpec as P

GROUP = 16
SP = ("sp_0", "sp_1")
SP_TP = ("sp_0", "sp_1", "tp")


HIGHEST = lax.Precision.HIGHEST


def from_everyone(array, axis):
    copies = jnp.broadcast_to(array, (lax.axis_size(axis), *array.shape))
    return lax.all_to_all(copies, axis, split_axis=0, concat_axis=0, tiled=True)


def all_in_one(array, axis):
    leaves = jax.tree.leaves(array)
    turns = sorted(range(len(leaves)), key=lambda k: -leaves[k].size)
    width = (1, *leaves[turns[0]].shape)[-1]
    lines = [
        jnp.pad(leaves[k].reshape(-1), (0, -leaves[k].size % width)).reshape(-1, width)
        for k in turns
    ]
    both, at, found = (from_everyone(jnp.concatenate(lines), axis), 0, {})
    for k, line in zip(turns, lines):
        section = both[:, at : at + len(line)].reshape(len(both), -1)
        found[k] = section[:, : leaves[k].size].reshape(-1, *leaves[k].shape)
        at += len(line)
    numbers = iter(range(len(leaves)))
    return jax.tree.map(lambda _: found[next(numbers)], array)


def folded_in_pairs(pieces, combine):
    while len(jax.tree.leaves(pieces)[0]) > 1:
        pieces = jax.vmap(combine)(
            *(jax.tree.map(lambda part: part[side::2], pieces) for side in (0, 1))
        )
    return jax.tree.map(lambda part: part[0], pieces)


def carried_in(array, axis, combine, identity, reverse):
    devices, here = (lax.axis_size(axis), lax.axis_index(axis))
    passed = jnp.arange(devices) > here if reverse else jnp.arange(devices) < here

    def kept(part, zero, own):
        part = jnp.where(
            passed.reshape(-1, *(1 for _ in own.shape)), part, jnp.asarray(zero, own.dtype)
        )
        return part[::-1] if reverse else part

    pieces = all_in_one(array, axis)
    return folded_in_pairs(jax.tree.map(kept, pieces, identity, array), combine)


def whole_of(array, axes, dim):
    for axis in reversed(axes):
        array = lax.all_gather(array, axis, axis=dim, tiled=True)
    return array


def split_up(array, dim, devices):
    before, after = (array.shape[:dim], array.shape[dim + 1 :])
    return jnp.moveaxis(array.reshape(*before, devices, -1, *after), dim, 0)


def summed_on_arrival(array, axis, dim):
    blocks = split_up(array, dim, lax.axis_size(axis))
    arrived = lax.all_to_all(blocks, axis, split_axis=0, concat_axis=0, tiled=True)
    return arrived.astype(jnp.float32).sum(axis=0)


def laid_out(blocks, dim):
    blocks = jnp.moveaxis(blocks, 0, dim)
    shape = blocks.shape
    return blocks.reshape(*shape[:dim], shape[dim] * shape[dim + 1], *shape[dim + 2 :])


def gather_directly(array, axis, dim):
    return laid_out(from_everyone(array, axis), dim)


def discretize(log_dt, decay_rate, frequency):
    step_size = jnp.exp(log_dt)[:, None]
    magnitude = jnp.exp(-step_size * decay_rate)
    angle_step = step_size * frequency
    state_real = magnitude * jnp.cos(angle_step)
    state_imag = magnitude * jnp.sin(angle_step)
    denominator = decay_rate * decay_rate + frequency * frequency
    shifted = state_real - 1.0
    zoh_real = (-shifted * decay_rate + state_imag * frequency) / denominator
    holdfixed_angle_part = (-state_imag * decay_rate - shifted * frequency) / denominator
    return (state_real, state_imag, zoh_real, holdfixed_angle_part)


def input_maps(zoh_real, holdfixed_angle_part, input_real, input_imag):
    scale_real = zoh_real[None, :, :, None]
    scale_imag = holdfixed_angle_part[None, :, :, None]
    return (
        scale_real * input_real - scale_imag * input_imag,
        scale_real * input_imag + scale_imag * input_real,
    )


def pair_combine(earlier, later):
    mult_one_real, mult_one_imag, first_state_real, state_one_imag = earlier
    mult_two_real, second_multiplier_imag, state_two_real, state_two_imag = later
    return (
        mult_two_real * mult_one_real - second_multiplier_imag * mult_one_imag,
        mult_two_real * mult_one_imag + second_multiplier_imag * mult_one_real,
        mult_two_real * first_state_real - second_multiplier_imag * state_one_imag + state_two_real,
        mult_two_real * state_one_imag + second_multiplier_imag * first_state_real + state_two_imag,
    )


def blocked_scan(mult_real, mult_imag, drive_real, drive_imag, reverse):
    tokens_here, width = mult_real.shape
    span = min(16, tokens_here)
    count = tokens_here // span
    block_mr, block_mi, block_dr, block_di = (
        item.reshape(count, span, width) for item in (mult_real, mult_imag, drive_real, drive_imag)
    )
    running_pr = jnp.ones((count, width), jnp.float32)
    running_pi = jnp.zeros((count, width), jnp.float32)
    running_sr = jnp.zeros((count, width), jnp.float32)
    running_si = jnp.zeros((count, width), jnp.float32)
    slots = [None] * span
    positions = range(span - 1, -1, -1) if reverse else range(span)
    for place in positions:
        step_real = block_mr[:, place]
        step_imag = block_mi[:, place]
        running_pr, running_pi = (
            step_real * running_pr - step_imag * running_pi,
            step_real * running_pi + step_imag * running_pr,
        )
        running_sr, running_si = (
            step_real * running_sr - step_imag * running_si + block_dr[:, place],
            step_real * running_si + step_imag * running_sr + block_di[:, place],
        )
        slots[place] = (running_pr, running_pi, running_sr, running_si)
    inner = tuple((jnp.stack([slot[member] for slot in slots], axis=1) for member in range(4)))
    edge = 0 if reverse else span - 1
    ends = tuple((item[:, edge] for item in inner))
    outer = lax.associative_scan(pair_combine, ends, reverse=reverse, axis=0)
    ones_row = jnp.ones((1, width), jnp.float32)
    zero_row = jnp.zeros((1, width), jnp.float32)
    neutral = (ones_row, zero_row, zero_row, zero_row)
    if reverse:
        carry = tuple(
            (jnp.concatenate([item[1:], blank], axis=0) for item, blank in zip(outer, neutral))
        )
    else:
        carry = tuple(
            (jnp.concatenate([blank, item[:-1]], axis=0) for item, blank in zip(outer, neutral))
        )
    carry_mr, carry_mi, carry_sr, carry_si = (item[:, None, :] for item in carry)
    inner_mr, inner_mi, inner_sr, inner_si = inner
    prod_real = inner_mr * carry_mr - inner_mi * carry_mi
    prod_imag = inner_mr * carry_mi + inner_mi * carry_mr
    local_real = inner_sr + inner_mr * carry_sr - inner_mi * carry_si
    local_imag = inner_si + inner_mr * carry_si + inner_mi * carry_sr
    return tuple(
        (
            item.reshape(tokens_here, width)
            for item in (prod_real, prod_imag, local_real, local_imag)
        )
    )


def chain_combine(earlier, later):
    early_real, early_imag, early_state_real, early_state_imag, early_near, early_far = earlier
    late_real, late_imag, late_state_real, late_state_imag, late_near, late_far = later
    joined = (late_near == early_far) | (early_far < 0.0) | (late_near < 0.0)
    linked = jnp.where(joined, 1.0, 0.0).astype(jnp.float32)
    step_real = linked * late_real
    step_imag = linked * late_imag
    return (
        step_real * early_real - step_imag * early_imag,
        step_real * early_imag + step_imag * early_real,
        step_real * early_state_real - step_imag * early_state_imag + late_state_real,
        step_real * early_state_imag + step_imag * early_state_real + late_state_imag,
        jnp.where(early_near < 0.0, late_near, early_near),
        jnp.where(late_far < 0.0, early_far, late_far),
    )


def direction_pass(
    grouped,
    doc_ids,
    keep_rates,
    state_real,
    state_imag,
    map_real,
    map_imag,
    read_real,
    read_imag,
    reverse,
):
    tokens_here, groups_here, group_width = grouped.shape
    states_here = state_real.shape[1]
    flat_width = groups_here * states_here
    drive_real = jnp.einsum("tgi,gpi->tgp", grouped, map_real, precision=HIGHEST).reshape(
        tokens_here, flat_width
    )
    drive_imag = jnp.einsum("tgi,gpi->tgp", grouped, map_imag, precision=HIGHEST).reshape(
        tokens_here, flat_width
    )
    same_doc = (doc_ids[1:] == doc_ids[:-1]).astype(jnp.float32)
    single = jnp.ones((1,), jnp.float32)
    doc_links = (
        jnp.concatenate([same_doc, single]) if reverse else jnp.concatenate([single, same_doc])
    )
    factor = keep_rates[:, :, None] * doc_links[:, None, None]
    mult_real = (factor * state_real[None]).reshape(tokens_here, flat_width)
    mult_imag = (factor * state_imag[None]).reshape(tokens_here, flat_width)
    prod_real, prod_imag, local_real, local_imag = blocked_scan(
        mult_real, mult_imag, drive_real, drive_imag, reverse
    )
    far_end = 0 if reverse else tokens_here - 1
    near_end = tokens_here - 1 if reverse else 0
    doc_values = doc_ids.astype(jnp.float32)
    summary = (
        prod_real[far_end],
        prod_imag[far_end],
        local_real[far_end],
        local_imag[far_end],
        doc_values[near_end],
        doc_values[far_end],
    )
    neutral = (
        jnp.ones((flat_width,), jnp.float32),
        jnp.zeros((flat_width,), jnp.float32),
        jnp.zeros((flat_width,), jnp.float32),
        jnp.zeros((flat_width,), jnp.float32),
        jnp.array(-1.0, jnp.float32),
        jnp.array(-1.0, jnp.float32),
    )
    carried = carried_in(summary, SP, chain_combine, neutral, reverse)
    joined = (doc_values[near_end] == carried[5]).astype(jnp.float32)
    enter_real = joined * carried[2]
    enter_imag = joined * carried[3]
    full_real = local_real + prod_real * enter_real[None] - prod_imag * enter_imag[None]
    full_imag = local_imag + prod_real * enter_imag[None] + prod_imag * enter_real[None]
    result = jnp.einsum(
        "tgp,gip->tgi",
        full_real.reshape(tokens_here, groups_here, states_here),
        read_real,
        precision=HIGHEST,
    )
    result = result - jnp.einsum(
        "tgp,gip->tgi",
        full_imag.reshape(tokens_here, groups_here, states_here),
        read_imag,
        precision=HIGHEST,
    )
    return result.reshape(tokens_here, groups_here * group_width)


def local(
    mix_input,
    stream,
    doc_ids,
    log_dt,
    decay_rate,
    frequency,
    input_real,
    input_imag,
    output_real,
    output_imag,
    skip_gain,
    log_keep,
    proj_weight,
    norm_gain,
    gate_weight,
    up_weight,
    down_weight,
):
    gate_whole, up_whole = (whole_of(gate_weight, SP, 0), whole_of(up_weight, SP, 0))
    down_whole = whole_of(down_weight, SP, 1)
    state_real, state_imag, zoh_real, holdfixed_angle_part = discretize(
        log_dt, decay_rate, frequency
    )
    map_real, map_imag = input_maps(zoh_real, holdfixed_angle_part, input_real, input_imag)
    tokens_here = mix_input.shape[0]
    channels = mix_input.astype(jnp.float32)
    grouped = channels.reshape(tokens_here, log_dt.shape[0], GROUP)
    keep_rates = jnp.exp(log_keep).T
    mixed_pre = skip_gain * channels
    for direction, reverse in ((0, False), (1, True)):
        mixed_pre = mixed_pre + direction_pass(
            grouped,
            doc_ids,
            keep_rates,
            state_real,
            state_imag,
            map_real[direction],
            map_imag[direction],
            output_real[direction],
            output_imag[direction],
            reverse,
        )
    mixed = jax.nn.gelu(mixed_pre).astype(jnp.bfloat16)
    branch = summed_on_arrival(
        jnp.dot(mixed, proj_weight, preferred_element_type=jnp.float32).astype(jnp.bfloat16),
        "tp",
        0,
    )
    resid = stream.astype(jnp.float32) + branch
    scale = lax.rsqrt(jnp.mean(resid * resid, axis=-1, keepdims=True) + 1e-06)
    normed = (resid * scale * norm_gain).astype(jnp.bfloat16)
    rows_all = gather_directly(normed, "tp", 0)
    gate = jnp.dot(rows_all, gate_whole, preferred_element_type=jnp.float32)
    upward = jnp.dot(rows_all, up_whole, preferred_element_type=jnp.float32)
    hidden = (jax.nn.silu(gate) * upward).astype(jnp.bfloat16)
    partial_out = jnp.dot(hidden, down_whole, preferred_element_type=jnp.float32)
    ffn = summed_on_arrival(partial_out.astype(jnp.bfloat16), "tp", 0)
    return (resid + 0.5 * ffn).astype(jnp.bfloat16)


def solution(mesh):
    torus = Mesh(mesh.devices.reshape(8, 4, mesh.shape["tp"]), ("sp_0", "sp_1", "tp"))
    in_specs = (
        P(SP, "tp"),
        P(SP_TP, None),
        P(SP),
        P("tp"),
        P("tp", None),
        P("tp", None),
        P(None, "tp", None, None),
        P(None, "tp", None, None),
        P(None, "tp", None, None),
        P(None, "tp", None, None),
        P("tp"),
        P("tp", SP),
        P("tp", None),
        P(),
        P(SP, "tp"),
        P(SP, "tp"),
        P("tp", SP),
    )
    out_specs = P(SP_TP, None)
    return jax.shard_map(local, mesh=torus, in_specs=in_specs, out_specs=out_specs, check_vma=False)
```

profile of v0, /device:TPU:1, one launch (start us, length us, event | category | flops | bytes accessed | tf_op | source)
XLA Modules:
  0.0 346.8 jit_solution(15707418047209030419)
XLA Ops:
  6.5 13.1 %all_gather.18 = bf16[256,704]{1,0:T(8,128)(2,1)} all-gather(bf16[64,704]{1,0:T(8,128)(2,1)} %param.31), channel_id=1, replica_groups=mesh['sp_0'=8,'sp_1'=4,'tp'=8] {'sp_1'}, dimensions={0}, use_global_device_ids=true | all-gather | bytes 450560 | tf_op jit(solution)/shard_map/all_gather | solution.py:61
  19.8 10.7 %all_gather.20 = bf16[256,704]{1,0:T(8,128)(2,1)} all-gather(bf16[64,704]{1,0:T(8,128)(2,1)} %param.32), channel_id=1, replica_groups=mesh['sp_0'=8,'sp_1'=4,'tp'=8] {'sp_1'}, dimensions={0}, use_global_device_ids=true | all-gather | bytes 450560 | tf_op jit(solution)/shard_map/all_gather | solution.py:61
  39.8 1.5 copy.610
  42.3 4.2 %fusion.208 = (f32[16,1,512]{2,1,0:T(1,128)}, f32[16,1,512]{2,1,0:T(1,128)}, f32[16,1,512]{2,1,0:T(1,128)}, f32[16,1,512]{2,1,0:T(1,128)}, f32[16,1,512]{2,1,0:T...) fusion(f32[16,16,512]{2,1,0:T(8,128)} %reshape_reshape.16), kind=kLoop, calls=%fused_computation.995 | loop fusion | bytes 1048576 | tf_op jit(solution)/shard_map/slice | solution.py:140
  51.7 1.8 copy_multiply_fusion.1
  69.3 2.2 constant_dynamic-update-slice_fusion.127
  71.5 1.4 constant_dynamic-update-slice_fusion.63
  72.9 1.2 convert_element_type.58
  78.5 1.3 multiply_subtract_fusion.43
  80.5 1.2 pad.544
  82.4 1.2 pad.347
  86.3 1.3 add_add_fusion.42
  88.4 1.2 pad.546
  91.0 1.4 subtract_add_fusion.36
  92.4 1.3 pad_maximum_fusion
  93.7 1.9 pad.343
  97.0 1.2 pad.545
  99.0 1.2 pad.345
  111.8 1.4 constant_dynamic-update-slice_fusion.79
  123.4 1.4 constant_dynamic-update-slice_fusion.62
  124.8 1.4 constant_dynamic-update-slice_fusion.61
  127.5 1.5 constant_dynamic-update-slice_fusion.58
  129.0 1.4 constant_dynamic-update-slice_fusion.57
  130.4 1.4 constant_dynamic-update-slice_fusion.56
  131.9 1.4 constant_dynamic-update-slice_fusion.55
  133.3 1.4 constant_dynamic-update-slice_fusion.54
  134.8 1.4 constant_dynamic-update-slice_fusion.53
  136.2 1.4 constant_dynamic-update-slice_fusion.52
  137.6 1.4 constant_dynamic-update-slice_fusion.51
  147.9 9.8 %all-to-all-start = ((f32[32,6,512]{2,1,0:T(8,128)}), f32[32,6,512]{2,1,0:T(8,128)}, u32[]{:S(2)}, u32[]{:S(2)}) async-start(f32[32,6,512]{2,1,0:T(8,128)} %broadcast_in_dim.148), calls=%async_computation | async-start | bytes 1048576 | tf_op jit(solution)/shard_map/all_to_all | solution.py:17
  157.8 11.6 %all_gather.22 = bf16[704,256]{0,1:T(8,128)(2,1)} all-gather(bf16[704,64]{0,1:T(8,128)(2,1)S(1)} %copy-done.121), channel_id=1, replica_groups=mesh['sp_0'=8,'sp_1'=4,'tp'=8] {'sp_1'}, dimensions={1}, use_global_device_ids=true | all-gather | bytes 450560 | tf_op jit(solution)/shard_map/all_gather | solution.py:61
  169.5 1.3 add.3562
  170.8 2.2 add.3565
  173.0 2.2 sub.1636
  175.2 1.2 sub.1642
  180.5 1.4 constant_dynamic-update-slice_fusion.125
  181.9 1.4 constant_dynamic-update-slice_fusion.124
  183.3 1.4 constant_dynamic-update-slice_fusion.123
  184.6 1.4 constant_dynamic-update-slice_fusion.122
  186.0 1.4 constant_dynamic-update-slice_fusion.121
  187.4 1.4 constant_dynamic-update-slice_fusion.120
  188.7 1.4 constant_dynamic-update-slice_fusion.119
  190.1 1.4 constant_dynamic-update-slice_fusion.118
  191.4 1.4 constant_dynamic-update-slice_fusion.117
  192.8 1.4 constant_dynamic-update-slice_fusion.116
  194.2 1.4 constant_dynamic-update-slice_fusion.115
  195.5 1.4 constant_dynamic-update-slice_fusion.114
  196.9 1.4 constant_dynamic-update-slice_fusion.113
  203.0 1.4 constant_dynamic-update-slice_fusion.64
  205.1 2.5 multiply_add_fusion.2
  207.9 1.2 sub.1738
  209.1 1.3 copy.698
  210.5 1.2 add.3765
  212.0 1.2 sub.1732
  216.7 9.6 %all-to-all-start.1 = ((f32[32,6,512]{2,1,0:T(8,128)}), f32[32,6,512]{2,1,0:T(8,128)S(1)}, u32[]{:S(2)}, u32[]{:S(2)}) async-start(f32[32,6,512]{2,1,0:T(8,128)} %broadcast_in_dim.157), calls=%async_computation.1 | async-start | bytes 1048576 | tf_op jit(solution)/shard_map/all_to_all | solution.py:17
  226.3 2.5 fusion.207
  231.4 1.5 fusion.23
  251.8 1.9 multiply_add_fusion.1
  258.7 1.9 multiply_add_fusion
  263.4 28.2 %all_to_all.25 = bf16[8,32,2048]{2,1,0:T(8,128)(2,1)S(1)} all-to-all(bf16[8,32,2048]{2,1,0:T(8,128)(2,1)S(1)} %bitcast.1396), channel_id=1, replica_groups=mesh['sp_0'=8,'sp_1'=4,'tp'=8] {'tp'}, dimensions={0} | all-to-all | bytes 2097152 | tf_op jit(solution)/shard_map/all_to_all | solution.py:72
  292.1 18.4 %all_to_all.26 = bf16[8,32,2048]{2,1,0:T(8,128)(2,1)S(1)} all-to-all(bf16[8,32,2048]{2,1,0:T(8,128)(2,1)S(1)} %broadcast_in_dim.159), channel_id=1, replica_groups=mesh['sp_0'=8,'sp_1'=4,'tp'=8] {'tp'}, dimensions={0} | all-to-all | bytes 2097152 | tf_op jit(solution)/shard_map/all_to_all | solution.py:17
  310.5 4.1 %fusion.216 = f32[256,704]{0,1:T(8,128)} fusion(bf16[256,2048]{1,0:T(8,128)(2,1)S(1)} %bitcast.1409, bf16[2048,704]{1,0:T(8,128)(2,1)} %all-gather.4.cloned.1.call-done), kind=kOutput, calls=%fused_computation.1011 | convolution fusion | flops 738197504 | bytes 4653056 | tf_op jit(solution)/shard_map/dot_general | solution.py:315
  314.6 6.4 %convolution_convert_fusion.1 = bf16[256,2048]{1,0:T(8,128)(2,1)S(1)} fusion(bf16[704,2048]{0,1:T(8,128)(2,1)} %all-gather.8.cloned.1.call-done, bf16[256,2048]{1,0:T(8,128)(2,1)S(1)} %bitcast.1410, bf16[2048,704]{1,0:T(8,128)(2,1)} %all-gather.6.cloned.1.call-done, f32[256,704]{0,1:T(8,128)} %fusion.216), kind=kOutput, calls=%fused_computation.1 | convolution fusion | flops 1478000640 | bytes 8585216 | tf_op jit(solution)/shard_map/dot_general | solution.py:318
  321.0 18.4 %all_to_all.27 = bf16[8,32,2048]{2,1,0:T(8,128)(2,1)S(1)} all-to-all(bf16[8,32,2048]{2,1,0:T(8,128)(2,1)S(1)} %bitcast.1411), channel_id=1, replica_groups=mesh['sp_0'=8,'sp_1'=4,'tp'=8] {'tp'}, dimensions={0} | all-to-all | bytes 2097152 | tf_op jit(solution)/shard_map/all_to_all | solution.py:72
  (813 shorter events, 107.7 us)
Async XLA Ops:
  6.5 256.4 %copy-start = (bf16[128,2048]{1,0:T(8,128)(2,1)S(1)}, bf16[128,2048]{1,0:T(8,128)(2,1)}, u32[]{:S(2)}) copy-start(bf16[128,2048]{1,0:T(8,128)(2,1)} %param.29) | copy-start | bytes 1572868
  6.5 30.0 %copy-start.122 = (s32[256]{0:T(256)S(1)}, s32[256]{0:T(256)}, u32[]{:S(2)}) copy-start(s32[256]{0:T(256)} %param.19) | copy-start | bytes 3076
  6.5 30.1 %copy-start.124 = (f32[8,256]{1,0:T(8,128)S(1)}, f32[8,256]{1,0:T(8,128)}, u32[]{:S(2)}) copy-start(f32[8,256]{1,0:T(8,128)} %param.28) | copy-start | bytes 24580
  6.5 304.0 %all-gather.4.cloned.1.call-start = ((), (), s32[]{:S(2)}) async-start(), calls=%async_computation.5 | async-start | bytes 3538944 | tf_op jit(solution)/shard_map/all_gather | solution.py:61
  19.7 294.9 %all-gather.6.cloned.1.call-start = ((), (), s32[]{:S(2)}) async-start(), calls=%async_computation.6 | async-start | bytes 3538944 | tf_op jit(solution)/shard_map/all_gather | solution.py:61
  53.5 73.3 %copy-start.1 = (f32[16,16,512]{2,0,1:T(8,128)}, f32[16,16,512]{2,0,1:T(8,128)S(1)}, u32[]{:S(2)}) copy-start(f32[16,16,512]{2,0,1:T(8,128)S(1)} %get-tuple-element.523) | copy-start | bytes 1572868
  53.5 73.3 %copy-start.3 = (f32[16,16,512]{2,0,1:T(8,128)}, f32[16,16,512]{2,0,1:T(8,128)S(1)}, u32[]{:S(2)}) copy-start(f32[16,16,512]{2,0,1:T(8,128)S(1)} %get-tuple-element.524) | copy-start | bytes 1572868
  56.4 11.4 %copy-start.106 = (f32[16,512]{1,0:T(8,128)}, f32[16,512]{1,0:T(8,128)S(1)}, u32[]{:S(2)}) copy-start(f32[16,512]{1,0:T(8,128)S(1)} %fusion.99) | copy-start | bytes 98308
  67.2 7.0 %copy-start.125 = (f32[1,512]{1,0:T(1,128)S(1)}, f32[1,512]{1,0:T(1,128)}, u32[]{:S(2)}) copy-start(f32[1,512]{1,0:T(1,128)} %get-tuple-element.509) | copy-start | bytes 6148
  67.2 7.0 %copy-start.126 = (f32[1,512]{1,0:T(1,128)S(1)}, f32[1,512]{1,0:T(1,128)}, u32[]{:S(2)}) copy-start(f32[1,512]{1,0:T(1,128)} %get-tuple-element.471) | copy-start | bytes 6148
  68.3 11.5 %slice-start = ((f32[16,512]{1,0:T(8,128)}), f32[1,512]{1,0:T(1,128)S(1)}, s32[]{:S(2)}) async-start(f32[16,512]{1,0:T(8,128)} %copy-done.106), calls=%async_computation.8 | async-start | bytes 4096 | tf_op jit(solution)/shard_map/slice | solution.py:147
  71.4 40.4 %copy-start.37 = (f32[16,1,512]{2,0,1:T(8,128)S(1)}, f32[16,1,512]{2,0,1:T(8,128)}, u32[]{:S(2)}) copy-start(f32[16,1,512]{2,0,1:T(8,128)} %get-tuple-element.147) | copy-start | bytes 98308
  71.4 40.4 %copy-start.38 = (f32[16,1,512]{2,0,1:T(8,128)S(1)}, f32[16,1,512]{2,0,1:T(8,128)}, u32[]{:S(2)}) copy-start(f32[16,1,512]{2,0,1:T(8,128)} %get-tuple-element.220) | copy-start | bytes 98308
  71.4 40.4 %copy-start.39 = (f32[16,1,512]{2,0,1:T(8,128)S(1)}, f32[16,1,512]{2,0,1:T(8,128)}, u32[]{:S(2)}) copy-start(f32[16,1,512]{2,0,1:T(8,128)} %get-tuple-element.221) | copy-start | bytes 98308
  71.5 51.9 %copy-start.54 = (f32[16,1,512]{2,1,0:T(1,128)S(1)}, f32[16,1,512]{2,1,0:T(1,128)}, u32[]{:S(2)}) copy-start(f32[16,1,512]{2,1,0:T(1,128)} %get-tuple-element.314) | copy-start | bytes 98308
  71.5 51.9 %copy-start.56 = (f32[16,1,512]{2,1,0:T(1,128)S(1)}, f32[16,1,512]{2,1,0:T(1,128)}, u32[]{:S(2)}) copy-start(f32[16,1,512]{2,1,0:T(1,128)} %get-tuple-element.329) | copy-start | bytes 98308
  72.9 54.5 %copy-start.83 = (f32[16,1,512]{2,1,0:T(1,128)S(1)}, f32[16,1,512]{2,1,0:T(1,128)}, u32[]{:S(2)}) copy-start(f32[16,1,512]{2,1,0:T(1,128)} %get-tuple-element.310) | copy-start | bytes 98308
  78.4 50.6 %copy-start.79 = (f32[16,1,512]{2,1,0:T(1,128)S(1)}, f32[16,1,512]{2,1,0:T(1,128)}, u32[]{:S(2)}) copy-start(f32[16,1,512]{2,1,0:T(1,128)} %get-tuple-element.309) | copy-start | bytes 98308
  80.5 50.0 %copy-start.75 = (f32[16,1,512]{2,1,0:T(1,128)S(1)}, f32[16,1,512]{2,1,0:T(1,128)}, u32[]{:S(2)}) copy-start(f32[16,1,512]{2,1,0:T(1,128)} %get-tuple-element.308) | copy-start | bytes 98308
  88.4 43.5 %copy-start.71 = (f32[16,1,512]{2,1,0:T(1,128)S(1)}, f32[16,1,512]{2,1,0:T(1,128)}, u32[]{:S(2)}) copy-start(f32[16,1,512]{2,1,0:T(1,128)} %get-tuple-element.307) | copy-start | bytes 98308
  88.4 43.5 %copy-start.81 = (f32[16,1,512]{2,1,0:T(1,128)S(1)}, f32[16,1,512]{2,1,0:T(1,128)}, u32[]{:S(2)}) copy-start(f32[16,1,512]{2,1,0:T(1,128)} %get-tuple-element.322) | copy-start | bytes 98308
  93.7 39.6 %copy-start.67 = (f32[16,1,512]{2,1,0:T(1,128)S(1)}, f32[16,1,512]{2,1,0:T(1,128)}, u32[]{:S(2)}) copy-start(f32[16,1,512]{2,1,0:T(1,128)} %get-tuple-element.306) | copy-start | bytes 98308
  93.7 39.6 %copy-start.77 = (f32[16,1,512]{2,1,0:T(1,128)S(1)}, f32[16,1,512]{2,1,0:T(1,128)}, u32[]{:S(2)}) copy-start(f32[16,1,512]{2,1,0:T(1,128)} %get-tuple-element.321) | copy-start | bytes 98308
  100.2 26.0 %copy-start.91 = (f32[16,1,512]{2,1,0:T(1,128)S(1)}, f32[16,1,512]{2,1,0:T(1,128)}, u32[]{:S(2)}) copy-start(f32[16,1,512]{2,1,0:T(1,128)} %get-tuple-element.312) | copy-start | bytes 98308
  100.2 26.0 %copy-start.98 = (f32[16,1,512]{2,1,0:T(1,128)S(1)}, f32[16,1,512]{2,1,0:T(1,128)}, u32[]{:S(2)}) copy-start(f32[16,1,512]{2,1,0:T(1,128)} %get-tuple-element.327) | copy-start | bytes 98308
  100.2 26.6 %copy-start.87 = (f32[16,1,512]{2,1,0:T(1,128)S(1)}, f32[16,1,512]{2,1,0:T(1,128)}, u32[]{:S(2)}) copy-start(f32[16,1,512]{2,1,0:T(1,128)} %get-tuple-element.311) | copy-start | bytes 98308
  100.2 26.6 %copy-start.96 = (f32[16,1,512]{2,1,0:T(1,128)S(1)}, f32[16,1,512]{2,1,0:T(1,128)}, u32[]{:S(2)}) copy-start(f32[16,1,512]{2,1,0:T(1,128)} %get-tuple-element.326) | copy-start | bytes 98308
  100.2 27.3 %copy-start.93 = (f32[16,1,512]{2,1,0:T(1,128)S(1)}, f32[16,1,512]{2,1,0:T(1,128)}, u32[]{:S(2)}) copy-start(f32[16,1,512]{2,1,0:T(1,128)} %get-tuple-element.325) | copy-start | bytes 98308
  100.2 28.8 %copy-start.89 = (f32[16,1,512]{2,1,0:T(1,128)S(1)}, f32[16,1,512]{2,1,0:T(1,128)}, u32[]{:S(2)}) copy-start(f32[16,1,512]{2,1,0:T(1,128)} %get-tuple-element.324) | copy-start | bytes 98308
  100.2 30.2 %copy-start.85 = (f32[16,1,512]{2,1,0:T(1,128)S(1)}, f32[16,1,512]{2,1,0:T(1,128)}, u32[]{:S(2)}) copy-start(f32[16,1,512]{2,1,0:T(1,128)} %get-tuple-element.323) | copy-start | bytes 98308
  101.1 33.7 %copy-start.63 = (f32[16,1,512]{2,1,0:T(1,128)S(1)}, f32[16,1,512]{2,1,0:T(1,128)}, u32[]{:S(2)}) copy-start(f32[16,1,512]{2,1,0:T(1,128)} %get-tuple-element.305) | copy-start | bytes 98308
  101.1 33.7 %copy-start.73 = (f32[16,1,512]{2,1,0:T(1,128)S(1)}, f32[16,1,512]{2,1,0:T(1,128)}, u32[]{:S(2)}) copy-start(f32[16,1,512]{2,1,0:T(1,128)} %get-tuple-element.320) | copy-start | bytes 98308
  104.9 31.3 %copy-start.61 = (f32[16,1,512]{2,1,0:T(1,128)S(1)}, f32[16,1,512]{2,1,0:T(1,128)}, u32[]{:S(2)}) copy-start(f32[16,1,512]{2,1,0:T(1,128)} %get-tuple-element.304) | copy-start | bytes 98308
  104.9 31.3 %copy-start.69 = (f32[16,1,512]{2,1,0:T(1,128)S(1)}, f32[16,1,512]{2,1,0:T(1,128)}, u32[]{:S(2)}) copy-start(f32[16,1,512]{2,1,0:T(1,128)} %get-tuple-element.319) | copy-start | bytes 98308
  110.3 27.4 %copy-start.59 = (f32[16,1,512]{2,1,0:T(1,128)S(1)}, f32[16,1,512]{2,1,0:T(1,128)}, u32[]{:S(2)}) copy-start(f32[16,1,512]{2,1,0:T(1,128)} %get-tuple-element.303) | copy-start | bytes 98308
  110.3 27.4 %copy-start.65 = (f32[16,1,512]{2,1,0:T(1,128)S(1)}, f32[16,1,512]{2,1,0:T(1,128)}, u32[]{:S(2)}) copy-start(f32[16,1,512]{2,1,0:T(1,128)} %get-tuple-element.318) | copy-start | bytes 98308
  113.2 26.7 %copy-start.13 = (f32[16,16,512]{2,0,1:T(8,128)}, f32[16,16,512]{2,0,1:T(8,128)S(1)}, u32[]{:S(2)}) copy-start(f32[16,16,512]{2,0,1:T(8,128)S(1)} %get-tuple-element.291) | copy-start | bytes 1572868
  113.2 25.8 %copy-start.115 = (f32[16,1,512]{2,0,1:T(8,128)S(1)}, f32[16,1,512]{2,0,1:T(8,128)}, u32[]{:S(2)}) copy-start(f32[16,1,512]{2,0,1:T(8,128)} %get-tuple-element.247) | copy-start | bytes 98308
  113.2 25.9 %copy-start.50 = (f32[16,1,512]{2,1,0:T(1,128)S(1)}, f32[16,1,512]{2,1,0:T(1,128)}, u32[]{:S(2)}) copy-start(f32[16,1,512]{2,1,0:T(1,128)} %get-tuple-element.302) | copy-start | bytes 98308
  113.2 25.9 %copy-start.52 = (f32[16,1,512]{2,1,0:T(1,128)S(1)}, f32[16,1,512]{2,1,0:T(1,128)}, u32[]{:S(2)}) copy-start(f32[16,1,512]{2,1,0:T(1,128)} %get-tuple-element.317) | copy-start | bytes 98308
  123.4 16.6 %copy-start.46 = (f32[16,1,512]{2,1,0:T(1,128)S(1)}, f32[16,1,512]{2,1,0:T(1,128)}, u32[]{:S(2)}) copy-start(f32[16,1,512]{2,1,0:T(1,128)} %get-tuple-element.301) | copy-start | bytes 98308
  123.4 16.6 %copy-start.48 = (f32[16,1,512]{2,1,0:T(1,128)S(1)}, f32[16,1,512]{2,1,0:T(1,128)}, u32[]{:S(2)}) copy-start(f32[16,1,512]{2,1,0:T(1,128)} %get-tuple-element.316) | copy-start | bytes 98308
  127.4 11.6 %copy-start.2 = (f32[16,16,512]{2,0,1:T(8,128)S(1)}, f32[16,16,512]{2,0,1:T(8,128)}, u32[]{:S(2)}) copy-start(f32[16,16,512]{2,0,1:T(8,128)} %copy-done.1) | copy-start | bytes 1572868
  127.5 11.7 %copy-start.4 = (f32[16,16,512]{2,0,1:T(8,128)S(1)}, f32[16,16,512]{2,0,1:T(8,128)}, u32[]{:S(2)}) copy-start(f32[16,16,512]{2,0,1:T(8,128)} %copy-done.3) | copy-start | bytes 1572868
  129.0 11.8 %copy-start.44 = (f32[16,1,512]{2,1,0:T(1,128)S(1)}, f32[16,1,512]{2,1,0:T(1,128)}, u32[]{:S(2)}) copy-start(f32[16,1,512]{2,1,0:T(1,128)} %get-tuple-element.300) | copy-start | bytes 98308
  129.0 11.8 %copy-start.102 = (f32[16,1,512]{2,1,0:T(1,128)S(1)}, f32[16,1,512]{2,1,0:T(1,128)}, u32[]{:S(2)}) copy-start(f32[16,1,512]{2,1,0:T(1,128)} %get-tuple-element.315) | copy-start | bytes 98308
  133.3 8.1 %copy-start.42 = (f32[16,1,512]{2,1,0:T(1,128)S(1)}, f32[16,1,512]{2,1,0:T(1,128)}, u32[]{:S(2)}) copy-start(f32[16,1,512]{2,1,0:T(1,128)} %get-tuple-element.299) | copy-start | bytes 98308
  142.9 14.9 %copy-start.121 = (bf16[704,64]{0,1:T(8,128)(2,1)S(1)}, bf16[704,64]{0,1:T(8,128)(2,1)}, u32[]{:S(2)}) copy-start(bf16[704,64]{0,1:T(8,128)(2,1)} %param.33) | copy-start | bytes 270340
  144.7 24.8 %copy-start.8 = (f32[16,16,512]{2,1,0:T(8,128)}, f32[16,16,512]{2,1,0:T(8,128)S(1)}, u32[]{:S(2)}) copy-start(f32[16,16,512]{2,1,0:T(8,128)S(1)} %copy.644) | copy-start | bytes 1572868
  145.0 24.5 %copy-start.10 = (f32[16,16,512]{2,1,0:T(8,128)}, f32[16,16,512]{2,1,0:T(8,128)S(1)}, u32[]{:S(2)}) copy-start(f32[16,16,512]{2,1,0:T(8,128)S(1)} %copy.649) | copy-start | bytes 1572868
  147.9 68.0 %all-to-all-start = ((f32[32,6,512]{2,1,0:T(8,128)}), f32[32,6,512]{2,1,0:T(8,128)}, u32[]{:S(2)}, u32[]{:S(2)}) async-start(f32[32,6,512]{2,1,0:T(8,128)} %broadcast_in_dim.148), calls=%async_computation | async-start | bytes 1048576 | tf_op jit(solution)/shard_map/all_to_all | solution.py:17
  157.7 156.8 %all-gather.8.cloned.1.call-start = ((), (), s32[]{:S(2)}) async-start(), calls=%async_computation.7 | async-start | bytes 3538944 | tf_op jit(solution)/shard_map/all_gather | solution.py:61
  176.6 26.2 %copy-start.113 = (f32[16,1,512]{2,0,1:T(8,128)S(1)}, f32[16,1,512]{2,0,1:T(8,128)}, u32[]{:S(2)}) copy-start(f32[16,1,512]{2,0,1:T(8,128)} %get-tuple-element.162) | copy-start | bytes 98308
  176.6 26.2 %copy-start.112 = (f32[16,1,512]{2,0,1:T(8,128)S(1)}, f32[16,1,512]{2,0,1:T(8,128)}, u32[]{:S(2)}) copy-start(f32[16,1,512]{2,0,1:T(8,128)} %get-tuple-element.163) | copy-start | bytes 98308
  176.6 26.3 %copy-start.111 = (f32[16,1,512]{2,0,1:T(8,128)S(1)}, f32[16,1,512]{2,0,1:T(8,128)}, u32[]{:S(2)}) copy-start(f32[16,1,512]{2,0,1:T(8,128)} %get-tuple-element.166) | copy-start | bytes 98308
  176.6 26.3 %copy-start.110 = (f32[16,1,512]{2,0,1:T(8,128)S(1)}, f32[16,1,512]{2,0,1:T(8,128)}, u32[]{:S(2)}) copy-start(f32[16,1,512]{2,0,1:T(8,128)} %get-tuple-element.167) | copy-start | bytes 98308
  176.6 26.3 %copy-start.109 = (f32[16,1,512]{2,0,1:T(8,128)S(1)}, f32[16,1,512]{2,0,1:T(8,128)}, u32[]{:S(2)}) copy-start(f32[16,1,512]{2,0,1:T(8,128)} %get-tuple-element.170) | copy-start | bytes 98308
  176.6 26.3 %copy-start.108 = (f32[16,1,512]{2,0,1:T(8,128)S(1)}, f32[16,1,512]{2,0,1:T(8,128)}, u32[]{:S(2)}) copy-start(f32[16,1,512]{2,0,1:T(8,128)} %get-tuple-element.171) | copy-start | bytes 98308
  176.7 26.3 %copy-start.107 = (f32[16,1,512]{2,0,1:T(8,128)S(1)}, f32[16,1,512]{2,0,1:T(8,128)}, u32[]{:S(2)}) copy-start(f32[16,1,512]{2,0,1:T(8,128)} %get-tuple-element.174) | copy-start | bytes 98308
  176.7 28.4 %copy-start.14 = (f32[16,16,512]{2,0,1:T(8,128)S(1)}, f32[16,16,512]{2,0,1:T(8,128)}, u32[]{:S(2)}) copy-start(f32[16,16,512]{2,0,1:T(8,128)} %copy-done.13) | copy-start | bytes 1572868
  216.7 23.5 %all-to-all-start.1 = ((f32[32,6,512]{2,1,0:T(8,128)}), f32[32,6,512]{2,1,0:T(8,128)S(1)}, u32[]{:S(2)}, u32[]{:S(2)}) async-start(f32[32,6,512]{2,1,0:T(8,128)} %broadcast_in_dim.157), calls=%async_computation.1 | async-start | bytes 1048576 | tf_op jit(solution)/shard_map/all_to_all | solution.py:17
  231.4 20.4 %copy-start.5 = (f32[256,8,64]{2,1,0:T(8,128)S(1)}, f32[256,8,64]{2,1,0:T(8,128)}, u32[]{:S(2)}) copy-start(f32[256,8,64]{2,1,0:T(8,128)} %add.3565) | copy-start | bytes 1572868
  261.7 30.0 %copy-start.12 = (bf16[32,2048]{1,0:T(8,128)(2,1)S(1)}, bf16[32,2048]{1,0:T(8,128)(2,1)}, u32[]{:S(2)}) copy-start(bf16[32,2048]{1,0:T(8,128)(2,1)} %param.18) | copy-start | bytes 393220
  262.8 29.1 %copy-start.123 = (f32[2048]{0:T(1024)S(1)}, f32[2048]{0:T(1024)}, u32[]{:S(2)}) copy-start(f32[2048]{0:T(1024)} %param.30) | copy-start | bytes 24580
  (71 other events, 209.2 us)
Sparse Core Ops, SparseCore 0:
  19.8 48.4 all-gather.3
  70.1 43.5 all-gather.5
  169.6 53.7 all-gather.7
where the time goes:
time: 353 us; the launch traced here: 347 us
  local copies, waits for them, and re-layouts  120 us (34%)
  blocking collectives  100 us (28%)
  other arithmetic  62.8 us (18%)
  between operations  26.2 us (7%)
  starting transfers between devices  19.5 us (6%)
  matrix products  17.8 us (5%)
    unnamed x330, local copies, waits for them, and re-layouts  49.8 us
    all_to_all x2, blocking collectives, summed_on_arrival(): lax.all_to_all(blocks, axis, split_axis=0, concat_axis=0, tiled=True)  46.6 us
    all_gather x3, blocking collectives, whole_of(): array = lax.all_gather(array, axis, axis=dim, tiled=True)  35.4 us
    unnamed x30, other arithmetic  23.3 us
    all_to_all x2, starting transfers between devices, from_everyone(): return lax.all_to_all(copies, axis, split_axis=0, concat_axis=0, tiled=True)  19.4 us
    all_to_all x1, blocking collectives, from_everyone(): return lax.all_to_all(copies, axis, split_axis=0, concat_axis=0, tiled=True)  18.4 us
    slice x112, local copies, waits for them, and re-layouts, folded_in_pairs(): part[side::2]  11.3 us
    slice x99, local copies, waits for them, and re-layouts, blocked_scan(): outer = lax.associative_scan(pair_combine, ends, reverse=reverse, axis=0)  10.7 us
  transfers between devices with their start and end apart: 5, of which 0 were waited for; matrix products, arithmetic and copies ran while one was open for 55% of the time, Pallas kernels for 0%

commit v1 on v0

v1 whole, which is shorter than its diff:
```python
import jax
import jax.numpy as jnp
from jax import lax
from jax.experimental import pallas as pl
from jax.experimental.pallas import tpu as pltpu
from jax.sharding import Mesh
from jax.sharding import PartitionSpec as P

GROUP = 16
SP = ("z", "y")
TP = ("x", "c")
HIGHEST = lax.Precision.HIGHEST


def discretize(log_dt, decay_rate, frequency):
    step_size = jnp.exp(log_dt)[:, None]
    magnitude = jnp.exp(-step_size * decay_rate)
    angle_step = step_size * frequency
    state_real = magnitude * jnp.cos(angle_step)
    state_imag = magnitude * jnp.sin(angle_step)
    denominator = decay_rate * decay_rate + frequency * frequency
    shifted = state_real - 1.0
    zoh_real = (-shifted * decay_rate + state_imag * frequency) / denominator
    zoh_imag = (-state_imag * decay_rate - shifted * frequency) / denominator
    return (state_real, state_imag, zoh_real, zoh_imag)


def input_maps(zoh_real, zoh_imag, input_real, input_imag):
    scale_real = zoh_real[None, :, :, None]
    scale_imag = zoh_imag[None, :, :, None]
    return (
        scale_real * input_real - scale_imag * input_imag,
        scale_real * input_imag + scale_imag * input_real,
    )


def on_ring(array, axis, shift):
    size = lax.axis_size(axis)
    return lax.ppermute(array, axis, [(i, (i + shift) % size) for i in range(size)])


def drive_matrix(map_real, map_imag):
    groups, states = map_real.shape[1:3]
    own = jnp.eye(groups, dtype=jnp.float32)[:, None, :, None]

    def spread(part):
        return (part[:, :, None, :] * own).reshape(groups, states, groups * GROUP)

    none = jnp.zeros((groups, states, groups * GROUP), jnp.float32)
    rows = []
    for part in (map_real, map_imag):
        rows.append(jnp.concatenate([spread(part[0]), none], axis=2))
        rows.append(jnp.concatenate([none, spread(part[1])], axis=2))
    return jnp.concatenate(rows, axis=1)


def read_matrix(read_real, read_imag):
    groups, width, states = read_real.shape[1:]
    own = jnp.eye(groups, dtype=jnp.float32)[:, :, None, None]
    none = jnp.zeros((groups, width, states), jnp.float32)

    def spread(part):
        return (part[:, None] * own).reshape(groups, groups * width, 4 * states)

    ahead = jnp.concatenate([read_real[0], none, -read_imag[0], none], axis=2)
    back = jnp.concatenate([none, read_real[1], none, -read_imag[1]], axis=2)
    return jnp.concatenate([spread(ahead), spread(back)], axis=1)


def flip_matrix(count, dtype):
    rows = lax.broadcasted_iota(jnp.int32, (count, count), 0)
    cols = lax.broadcasted_iota(jnp.int32, (count, count), 1)
    return jnp.where(rows + cols == count - 1, 1.0, 0.0).astype(dtype)


def times_transposed(left, right, precision=None):
    return lax.dot_general(
        left,
        right,
        (((1,), (1,)), ((), ())),
        precision=precision,
        preferred_element_type=jnp.float32,
    )


def local_states_kernel(
    u_ref, factor_ref, drive_ref, pole_ref, docs_ref, real_ref, imag_ref, decay_ref, summary_ref
):
    tokens, channels = u_ref.shape
    groups, lanes = pole_ref.shape[1:]
    u = u_ref[...]
    backward = jnp.dot(
        flip_matrix(tokens, jnp.bfloat16), u, preferred_element_type=jnp.float32
    ).astype(jnp.bfloat16)
    both = jnp.concatenate([u, backward], axis=1)
    ahead = lax.broadcasted_iota(jnp.int32, (tokens, lanes), 1) < lanes // 2
    for g in range(groups):
        whole = drive_ref[g]
        first = whole.astype(jnp.bfloat16)
        rest = whole - first.astype(jnp.float32)
        second = rest.astype(jnp.bfloat16)
        third = (rest - second.astype(jnp.float32)).astype(jnp.bfloat16)
        drive = times_transposed(both, first)
        drive = drive + times_transposed(both, second)
        drive = drive + times_transposed(both, third)
        real_ref[:, g, :] = drive[:, :lanes]
        imag_ref[:, g, :] = drive[:, lanes:]
        decay_ref[:, g, :] = jnp.where(
            ahead, factor_ref[:, g : g + 1], factor_ref[:, groups + g : groups + g + 1]
        )
    pole_real, pole_imag = (pole_ref[0], pole_ref[1])

    def step(t, carry):
        state_real, state_imag, product = carry
        factor = decay_ref[t]
        step_real, step_imag = (factor * pole_real, factor * pole_imag)
        return (
            step_real * state_real - step_imag * state_imag + real_ref[t],
            step_real * state_imag + step_imag * state_real + imag_ref[t],
            product * factor,
        )

    zero = jnp.zeros((groups, lanes), jnp.float32)
    state_real, state_imag, product = lax.fori_loop(
        0, tokens, step, (zero, zero, zero + 1.0), unroll=8
    )
    summary_ref[0] = state_real
    summary_ref[1] = state_imag
    summary_ref[2] = product
    summary_ref[3] = docs_ref[...]


def mixing_kernel(
    place_ref,
    all_ref,
    u_ref,
    real_ref,
    imag_ref,
    decay_ref,
    pole_ref,
    docs_ref,
    read_ref,
    skip_ref,
    out_ref,
    state_real_ref,
    state_imag_ref,
    mixed_ref,
):
    tokens, channels = u_ref.shape
    groups, lanes = pole_ref.shape[1:]
    blocks = all_ref.shape[0]
    here = place_ref[0]
    pole_real, pole_imag = (pole_ref[0], pole_ref[1])
    far_real, far_imag = (pole_real, pole_imag)
    for _ in range(tokens.bit_length() - 1):
        far_real, far_imag = (far_real * far_real - far_imag * far_imag, 2.0 * far_real * far_imag)
    ahead = lax.broadcasted_iota(jnp.int32, (groups, lanes), 1) < lanes // 2

    def near_of(code):
        return jnp.floor(code * 0.125)

    def join(j, carry):
        state_real, state_imag, last = carry
        other = blocks - 1 - j
        local_real, local_imag, product, code = (
            jnp.where(ahead, all_ref[j, k], all_ref[other, k]) for k in range(4)
        )
        before = jnp.where(ahead, jnp.where(j < here, 1, 0), jnp.where(other > here, 1, 0)) > 0
        near = near_of(code)
        kept = jnp.where(near == last, product, 0.0)
        next_real = kept * (far_real * state_real - far_imag * state_imag) + local_real
        next_imag = kept * (far_real * state_imag + far_imag * state_real) + local_imag
        return (
            jnp.where(before, next_real, state_real),
            jnp.where(before, next_imag, state_imag),
            jnp.where(before, code - 8.0 * near, last),
        )

    zero = jnp.zeros((groups, lanes), jnp.float32)
    enter_real, enter_imag, last = lax.fori_loop(0, blocks - 1, join, (zero, zero, zero - 1.0))
    joined = near_of(docs_ref[...]) == last
    enter_real = jnp.where(joined, enter_real, 0.0)
    enter_imag = jnp.where(joined, enter_imag, 0.0)

    def step(t, carry):
        state_real, state_imag = carry
        factor = decay_ref[t]
        step_real, step_imag = (factor * pole_real, factor * pole_imag)
        next_real = step_real * state_real - step_imag * state_imag + real_ref[t]
        next_imag = step_real * state_imag + step_imag * state_real + imag_ref[t]
        state_real_ref[t] = next_real
        state_imag_ref[t] = next_imag
        return (next_real, next_imag)

    lax.fori_loop(0, tokens, step, (enter_real, enter_imag), unroll=8)
    read = jnp.zeros((tokens, 2 * channels), jnp.float32)
    for g in range(groups):
        states = jnp.concatenate([state_real_ref[:, g, :], state_imag_ref[:, g, :]], axis=1)
        read = read + times_transposed(states, read_ref[g], HIGHEST)
    backward = jnp.dot(
        flip_matrix(tokens, jnp.float32),
        read[:, channels:],
        precision=HIGHEST,
        preferred_element_type=jnp.float32,
    )
    pre = read[:, :channels] + backward + skip_ref[...] * u_ref[...].astype(jnp.float32)
    mixed_ref[...] = jax.nn.gelu(pre)
    rows = tokens // 8
    for k in range(8):
        start = pl.multiple_of(place_ref[1 + k] * rows, rows)
        out_ref[k * rows : (k + 1) * rows, :] = mixed_ref[pl.ds(start, rows), :].astype(
            jnp.bfloat16
        )


def feed_forward_kernel(
    rows_ref, gate_ref, up_ref, down_ref, keep_ref, send_ref, gate_acc, up_acc, hidden_ref
):
    i = pl.program_id(0)
    half = pl.num_programs(0) // 2
    shards, depth, hidden = gate_ref.shape

    @pl.when(i == 0)
    def _():
        gate_acc[...] = jnp.zeros(gate_acc.shape, jnp.float32)
        up_acc[...] = jnp.zeros(up_acc.shape, jnp.float32)

    @pl.when(i < half)
    def _():
        rows = rows_ref[...]
        gate_acc[...] += jnp.dot(
            rows,
            gate_ref[...].reshape(shards * depth, hidden),
            preferred_element_type=jnp.float32,
        )
        up_acc[...] += jnp.dot(
            rows, up_ref[...].reshape(shards * depth, hidden), preferred_element_type=jnp.float32
        )

    @pl.when(i == half - 1)
    def _():
        gate = gate_acc[...]
        hidden_ref[...] = (gate / (1.0 + jnp.exp(-gate)) * up_acc[...]).astype(jnp.bfloat16)

    @pl.when(i >= half)
    def _():
        made = times_transposed(
            hidden_ref[...], down_ref[...].reshape(shards * depth, hidden)
        )
        near = keep_ref.shape[0]
        keep_ref[...] = made[:near]
        send_ref[...] = made[near:].astype(jnp.bfloat16)


def feed_forward(rows, weights):
    tokens, features = rows.shape
    blocks, depth, hidden = weights.shape
    depth //= 3
    shards = 8
    half = blocks // shards
    width = shards * depth
    near = tokens // 2

    def weight_spec(which):
        if which < 2:
            return pl.BlockSpec(
                (shards, depth, hidden), lambda i: (jnp.minimum(i, half - 1), which, 0)
            )
        return pl.BlockSpec((shards, depth, hidden), lambda i: (jnp.maximum(i - half, 0), which, 0))

    return pl.pallas_call(
        feed_forward_kernel,
        grid=(2 * half,),
        in_specs=[
            pl.BlockSpec((tokens, width), lambda i: (0, jnp.minimum(i, half - 1))),
            weight_spec(0),
            weight_spec(1),
            weight_spec(2),
        ],
        out_specs=[
            pl.BlockSpec((near, width), lambda i: (0, jnp.maximum(i - half, 0))),
            pl.BlockSpec((near, width), lambda i: (0, jnp.maximum(i - half, 0))),
        ],
        out_shape=[
            jax.ShapeDtypeStruct((near, features), jnp.float32),
            jax.ShapeDtypeStruct((near, features), jnp.bfloat16),
        ],
        scratch_shapes=[
            pltpu.VMEM((tokens, hidden), jnp.float32),
            pltpu.VMEM((tokens, hidden), jnp.float32),
            pltpu.VMEM((tokens, hidden), jnp.bfloat16),
        ],
        name="feed_forward",
    )(rows, weights, weights, weights)


def summed_over_tp(keep, send):
    pair = keep + on_ring(send, "c", 1).astype(jnp.float32)
    chips = lax.axis_size("x")
    rows = pair.shape[0] // chips
    total = pair[:rows]
    away = pair.astype(jnp.bfloat16)
    for k in range(1, chips):
        arrived = on_ring(away[k * rows : (k + 1) * rows], "x", -k)
        total = total + arrived.astype(jnp.float32)
    return total


def rows_of_tp(array):
    chips = lax.axis_size("x")
    mine = jnp.concatenate([array] + [on_ring(array, "x", k) for k in range(1, chips)], axis=0)
    return jnp.concatenate([mine, on_ring(mine, "c", 1)], axis=0)


def local(
    mix_input,
    stream,
    doc_ids,
    log_dt,
    decay_rate,
    frequency,
    input_real,
    input_imag,
    output_real,
    output_imag,
    skip_gain,
    log_keep,
    proj_weight,
    norm_gain,
    gate_weight,
    up_weight,
    down_weight,
):
    weights = lax.all_gather(
        jnp.concatenate([gate_weight, up_weight, down_weight.T], axis=0), SP, axis=0, tiled=False
    )
    blocks = lax.axis_size(SP)
    chips = lax.axis_size("x")
    here, chip, core = (lax.axis_index(SP), lax.axis_index("x"), lax.axis_index("c"))
    tokens, channels = mix_input.shape
    groups, states = decay_rate.shape
    state_real, state_imag, zoh_real, zoh_imag = discretize(log_dt, decay_rate, frequency)
    map_real, map_imag = input_maps(zoh_real, zoh_imag, input_real, input_imag)
    drive = drive_matrix(map_real, map_imag)
    reader = read_matrix(output_real, output_imag)
    poles = jnp.stack([jnp.concatenate([part, part], axis=1) for part in (state_real, state_imag)])
    same_doc = (doc_ids[1:] == doc_ids[:-1]).astype(jnp.float32)
    single = jnp.ones((1,), jnp.float32)
    keep_rates = jnp.exp(log_keep)
    factors = jnp.concatenate(
        [
            (keep_rates * jnp.concatenate([single, same_doc])).T,
            (keep_rates * jnp.concatenate([same_doc, single])).T[::-1],
        ],
        axis=1,
    )
    first_doc, last_doc = (doc_ids[0].astype(jnp.float32), doc_ids[-1].astype(jnp.float32))
    ahead = lax.broadcasted_iota(jnp.int32, (groups, 2 * states), 1) < states
    docs = jnp.where(ahead, 8.0 * first_doc + last_doc, 8.0 * last_doc + first_doc)
    lanes = 2 * states
    by_token = jax.ShapeDtypeStruct((tokens, groups, lanes), jnp.float32)
    drive_real, drive_imag, decays, summary = pl.pallas_call(
        local_states_kernel,
        out_shape=[by_token] * 3 + [jax.ShapeDtypeStruct((4, groups, lanes), jnp.float32)],
        name="local_states",
    )(mix_input, factors, drive, poles, docs)
    everyone = lax.all_to_all(
        jnp.broadcast_to(summary, (blocks, *summary.shape)),
        SP,
        split_axis=0,
        concat_axis=0,
        tiled=True,
    )
    order = [
        2 * ((chip - k) % chips) + (core if own else 1 - core)
        for own in (True, False)
        for k in range(4)
    ]
    place = jnp.stack([here, *order]).astype(jnp.int32)
    vmem = pl.BlockSpec(memory_space=pltpu.VMEM)
    mixed = pl.pallas_call(
        mixing_kernel,
        out_shape=jax.ShapeDtypeStruct((tokens, channels), jnp.bfloat16),
        in_specs=[pl.BlockSpec(memory_space=pltpu.SMEM)] + [vmem] * 9,
        scratch_shapes=[
            pltpu.VMEM((tokens, groups, lanes), jnp.float32),
            pltpu.VMEM((tokens, groups, lanes), jnp.float32),
            pltpu.VMEM((tokens, channels), jnp.float32),
        ],
        name="mixing",
    )(
        place,
        everyone,
        mix_input,
        drive_real,
        drive_imag,
        decays,
        poles,
        docs,
        reader,
        skip_gain[None],
    )
    product = jnp.dot(mixed, proj_weight, preferred_element_type=jnp.float32)
    branch = summed_over_tp(product[: tokens // 2], product[tokens // 2 :].astype(jnp.bfloat16))
    resid = stream.astype(jnp.float32) + branch
    scale = lax.rsqrt(jnp.mean(resid * resid, axis=-1, keepdims=True) + 1e-06)
    normed = (resid * scale * norm_gain).astype(jnp.bfloat16)
    ffn = summed_over_tp(*feed_forward(rows_of_tp(normed), weights))
    return (resid + 0.5 * ffn).astype(jnp.bfloat16)


def solution(mesh):
    torus = Mesh(mesh.devices.reshape(8, 4, 4, 2), ("z", "y", "x", "c"))
    everything = SP + TP
    in_specs = (
        P(SP, TP),
        P(everything, None),
        P(SP),
        P(TP),
        P(TP, None),
        P(TP, None),
        P(None, TP, None, None),
        P(None, TP, None, None),
        P(None, TP, None, None),
        P(None, TP, None, None),
        P(TP),
        P(TP, SP),
        P(TP, None),
        P(),
        P(SP, TP),
        P(SP, TP),
        P(TP, SP),
    )
    return jax.shard_map(
        local, mesh=torus, in_specs=in_specs, out_specs=P(everything, None), check_vma=False
    )
```

time: 353 us -> 153 us (0.43); the launches traced: 347 us -> 153 us
  local copies, waits for them, and re-layouts: 120 us -> 6.4 us
  blocking collectives: 100 us -> 0 us
  waiting for transfers between devices: 0.06 us -> 65.3 us
  other arithmetic: 62.8 us -> 11.3 us
  Pallas kernels: 0 us -> 24.5 us
  matrix products: 17.8 us -> 1.26 us
  between operations: 26.2 us -> 15 us
  starting transfers between devices: 19.5 us -> 29.1 us
    all_to_all x3 -> x0, blocking collectives: 65 us -> none  [the longest x2 46.6 us: summed_on_arrival(): lax.all_to_all(blocks, axis, split_axis=0, concat_axis=0, tiled=True)]
    unnamed x330 -> x21, local copies, waits for them, and re-layouts: 49.8 us -> 0.88 us
    slice x242 -> x4, local copies, waits for them, and re-layouts: 37.7 us -> 0.74 us  [the longest x1 0.62 us: local(): doc_ids[0].astype(jnp.float32)]
    all_gather x3 -> x0, blocking collectives: 35.4 us -> none  [whole_of(): array = lax.all_gather(array, axis, axis=dim, tiled=True)]
    pallas_call x0 -> x3, Pallas kernels: none -> 24.5 us  [the longest x1 9.57 us: feed_forward(): pl.pallas_call(feed_forward_kernel, grid=(2 * half,), in_specs=[pl.BlockS...]
    ppermute x0 -> x12, waiting for transfers between devices: none -> 24.1 us  [on_ring(): lax.ppermute(array, axis, [(i, (i + shift) % size) for i in range(size)])]
    unnamed x30 -> x1, other arithmetic: 23.3 us -> 0.1 us
    all_gather x3 -> x1, waiting for transfers between devices: 0.01 us -> 23 us  [local(): lax.all_gather(jnp.concatenate([gate_weight, up_weight, down_weight.T], a...]
  transfers between devices with their start and end apart: 5 -> 14, of which waited for: 0 -> 12; matrix products, arithmetic and copies ran while one was open for 55% -> 9% of each run, Pallas kernels for 0% -> 10%
where the time goes in v1:
time: 153 us
  waiting for transfers between devices  65.3 us (43%)
  starting transfers between devices  29.1 us (19%)
  Pallas kernels  24.5 us (16%)
  between operations  15 us (10%)
  other arithmetic  11.3 us (7%)
  local copies, waits for them, and re-layouts  6.4 us (4%)
    ppermute x12, waiting for transfers between devices, on_ring(): lax.ppermute(array, axis, [(i, (i + shift) % size) for i in range(size)])  24.1 us
    all_gather x1, waiting for transfers between devices, local(): lax.all_gather(jnp.concatenate([gate_weight, up_weight, down_weight.T], a...  23 us
    all_to_all x1, waiting for transfers between devices, local(): lax.all_to_all(jnp.broadcast_to(summary, (blocks, *summary.shape)), SP, s...  18.2 us
    ppermute x12, starting transfers between devices, on_ring(): lax.ppermute(array, axis, [(i, (i + shift) % size) for i in range(size)])  17.1 us
    all_to_all x1, starting transfers between devices, local(): lax.all_to_all(jnp.broadcast_to(summary, (blocks, *summary.shape)), SP, s...  12 us
    pallas_call x1, Pallas kernels, feed_forward(): pl.pallas_call(feed_forward_kernel, grid=(2 * half,), in_specs=[pl.BlockS...  9.57 us
    pallas_call x1, Pallas kernels, local(): pl.pallas_call(mixing_kernel, out_shape=jax.ShapeDtypeStruct((tokens, cha...  8.09 us
    pallas_call x1, Pallas kernels, local(): pl.pallas_call(local_states_kernel, out_shape=[by_token] * 3 + [jax.Shape...  6.86 us
  transfers between devices with their start and end apart: 14, of which 12 were waited for; matrix products, arithmetic and copies ran while one was open for 9% of the time, Pallas kernels for 10%

profile of v1, /device:TPU:1, one launch (start us, length us, event | category | flops | bytes accessed | tf_op | source)
XLA Modules:
  0.0 152.9 jit_solution(16081900301769791296)
XLA Ops:
  6.5 1.8 %pad_maximum_fusion.2 = bf16[192,704]{1,0:T(8,128)(2,1)} fusion(bf16[64,704]{1,0:T(8,128)(2,1)} %bitcast.55, bf16[64,704]{1,0:T(8,128)(2,1)} %param.32, bf16[64,704]{1,0:T(8,128)(2,1)} %param.31), kind=kLoop, calls=%fused_computation.18 | loop fusion | flops 811008 | bytes 540672 | tf_op jit(solution)/shard_map/concatenate | solution.py:335
  8.3 0.0 all-gather.3.cloned.1.call-update
  8.3 0.7 exponential_negate_fusion
  9.0 0.8 cosine_multiply_fusion
  9.8 1.0 multiply_subtract_fusion
  10.9 0.2 copy.34
  11.1 0.0 copy-start.6
  11.2 0.2 copy.35
  11.4 0.2 copy.36
  11.6 0.2 copy.37
  11.8 0.1 mul.290
  11.9 0.1 mul.291
  12.0 0.6 fusion.17
  13.9 0.1 compare_convert_fusion
  13.9 0.1 pad_maximum_fusion.7
  14.0 0.2 rev.3
  14.2 0.8 copy.38.factor_ref
  15.0 0.1 maximum_bitcast_fusion
  15.0 0.6 pad_maximum_fusion.6.pole_ref
  15.6 0.1 broadcast_multiply_fusion.3
  15.7 1.5 select_maximum_fusion.drive_ref
  17.3 0.6 iota.51.docs_ref
  17.9 6.9 %local_states.1 = (f32[256,8,128]{2,1,0:T(8,128)}, f32[256,8,128]{2,1,0:T(8,128)}, f32[256,8,128]{2,1,0:T(8,128)}, f32[4,8,128]{2,1,0:T(8,128)}) custom-call(bf16[256,128]{1,0:T(8,128)(2,1)} %u_ref.3, f32[256,16]{1,0:T(8,128)} %copy.38.factor_ref, f32[8,256,256]{2,1,0:T(8,128)} %select_maximum_fusion.drive_ref, f32[2,8,128]{2,1,0:T(8,128)} %pad_maximum_fusion.6.pole_ref, ...), custom_call_target="tpu_custom_call" | custom-call | tf_op jit(solution)/shard_map/local_states/pallas_call | solution.py:362
  24.7 1.6 %broadcast_in_dim.16 = f32[32,4,8,128]{3,2,1,0:T(8,128)} broadcast(f32[4,8,128]{2,1,0:T(8,128)} %get-tuple-element.11), dimensions={1,2,3} | broadcast | bytes 540672 | tf_op jit(solution)/shard_map/broadcast_in_dim | solution.py:368
  26.3 12.0 %all-to-all-start = ((f32[32,4,8,128]{3,2,1,0:T(8,128)}), f32[32,4,8,128]{3,2,1,0:T(8,128)S(1)}, u32[]{:S(2)}, u32[]{:S(2)}) async-start(f32[32,4,8,128]{3,2,1,0:T(8,128)} %broadcast_in_dim.16), calls=%async_computation | async-start | bytes 1048576 | tf_op jit(solution)/shard_map/all_to_all | solution.py:367
  38.5 0.2 pad_maximum_fusion.3
  38.6 0.2 bitcast_multiply_fusion.1
  38.9 0.6 stack.48.place_ref
  39.5 1.6 %pad_maximum_fusion.read_ref = f32[8,256,256]{2,1,0:T(8,128)} fusion(f32[8,128,256]{2,1,0:T(8,128)S(1)} %get-tuple-element.50, f32[8,128,256]{2,1,0:T(8,128)S(1)} %get-tuple-element.49), kind=kLoop, calls=%fused_computation.9 | loop fusion | flops 524288 | bytes 4194304 | tf_op jit(solution)/shard_map/concatenate | solution.py:67
  41.0 18.2 %all-to-all-done.all_ref = f32[32,4,8,128]{3,2,1,0:T(8,128)S(1)} async-done(((f32[32,4,8,128]{3,2,1,0:T(8,128)}), f32[32,4,8,128]{3,2,1,0:T(8,128)S(1)}, u32[]{:S(2)}, u32[]{:S(2)}) %all-to-all-start) | async-done | bytes 524320 | tf_op jit(solution)/shard_map/all_to_all | solution.py:367
  59.2 0.8 copy-done.1
  60.0 8.1 %mixing.1 = bf16[256,128]{1,0:T(8,128)(2,1)} custom-call(s32[9]{0:T(128)} %stack.48.place_ref, f32[32,4,8,128]{3,2,1,0:T(8,128)} %copy-done.1, bf16[256,128]{1,0:T(8,128)(2,1)} %u_ref.3, f32[256,8,128]{2,1,0:T(8,128)} %get-tuple-element.12.real_ref, f32[256,8,128]{2,1,0:T(8,128)} %get-tuple-element.13.imag_ref, f32[256,8,128]{2,1,0:T(8,128)} %get-tuple-element.14.decay_ref, ...), custom_call_target="tpu_custom_call" | custom-call | tf_op jit(solution)/shard_map/mixing/pallas_call | solution.py:381
  68.1 1.3 fusion.18
  69.4 0.1 slice.133
  69.4 0.0 copy-start.5
  69.5 2.2 %collective-permute-start = (bf16[128,2048]{1,0:T(8,128)(2,1)S(1)}, bf16[128,2048]{1,0:T(8,128)(2,1)S(1)}, u32[]{:S(2)}, u32[]{:S(2)}) collective-permute-start(bf16[128,2048]{1,0:T(8,128)(2,1)S(1)} %slice.133), channel_id=1, source_target_pairs={{0,1},{1,0},{2,3},{3,2},{4,5},{5,4},{6,7},{7,6},{8,9},{9,8},{10,11... | collective-permute-start | bytes 1572872 | tf_op jit(solution)/shard_map/ppermute | solution.py:39
  71.7 1.5 %collective-permute-done = bf16[128,2048]{1,0:T(8,128)(2,1)S(1)} collective-permute-done((bf16[128,2048]{1,0:T(8,128)(2,1)S(1)}, bf16[128,2048]{1,0:T(8,128)(2,1)S(1)}, u32[]{:S(2)}, u32[]{:S(2)}) %collective-permute-start) | collective-permute-done | bytes 524320 | tf_op jit(solution)/shard_map/ppermute | solution.py:39
  73.2 0.2 fusion.14
  73.4 2.5 %collective-permute-start.1 = (bf16[32,2048]{1,0:T(8,128)(2,1)S(1)}, bf16[32,2048]{1,0:T(8,128)(2,1)S(1)}, u32[]{:S(2)}, u32[]{:S(2)}) collective-permute-start(bf16[32,2048]{1,0:T(8,128)(2,1)S(1)} %get-tuple-element.28), channel_id=1, source_target_pairs={{0,6},{2,0},{4,2},{6,4},{1,7},{3,1},{5,3},{7,5},{8,14},{10,8},{12,... | collective-permute-start | bytes 393224 | tf_op jit(solution)/shard_map/ppermute | solution.py:39
  75.9 0.5 collective-permute-start.2
  76.4 0.6 collective-permute-start.3
  77.0 2.0 %collective-permute-done.1 = bf16[32,2048]{1,0:T(8,128)(2,1)S(1)} collective-permute-done((bf16[32,2048]{1,0:T(8,128)(2,1)S(1)}, bf16[32,2048]{1,0:T(8,128)(2,1)S(1)}, u32[]{:S(2)}, u32[]{:S(2)}) %collective-permute-start.1) | collective-permute-done | bytes 131104 | tf_op jit(solution)/shard_map/ppermute | solution.py:39
  79.0 2.8 %collective-permute-done.2 = bf16[32,2048]{1,0:T(8,128)(2,1)S(1)} collective-permute-done((bf16[32,2048]{1,0:T(8,128)(2,1)S(1)}, bf16[32,2048]{1,0:T(8,128)(2,1)S(1)}, u32[]{:S(2)}, u32[]{:S(2)}) %collective-permute-start.2) | collective-permute-done | bytes 131104 | tf_op jit(solution)/shard_map/ppermute | solution.py:39
  81.8 3.9 %collective-permute-done.3 = bf16[32,2048]{1,0:T(8,128)(2,1)S(1)} collective-permute-done((bf16[32,2048]{1,0:T(8,128)(2,1)S(1)}, bf16[32,2048]{1,0:T(8,128)(2,1)S(1)}, u32[]{:S(2)}, u32[]{:S(2)}) %collective-permute-start.3) | collective-permute-done | bytes 131104 | tf_op jit(solution)/shard_map/ppermute | solution.py:39
  85.8 0.2 multiply_reduce_fusion
  86.0 0.1 constant_dynamic-update-slice_fusion.4
  86.1 0.3 collective-permute-start.4
  86.3 0.4 collective-permute-start.5
  86.8 2.2 %collective-permute-start.6 = (bf16[32,2048]{1,0:T(8,128)(2,1)S(1)}, bf16[32,2048]{1,0:T(8,128)(2,1)S(1)}, u32[]{:S(2)}, u32[]{:S(2)}) collective-permute-start(bf16[32,2048]{1,0:T(8,128)(2,1)S(1)} %get-tuple-element.20), channel_id=1, source_target_pairs={{0,6},{2,0},{4,2},{6,4},{1,7},{3,1},{5,3},{7,5},{8,14},{10,8},{12,... | collective-permute-start | bytes 393224 | tf_op jit(solution)/shard_map/ppermute | solution.py:39
  89.0 6.3 %collective-permute-done.4 = bf16[32,2048]{1,0:T(8,128)(2,1)S(1)} collective-permute-done((bf16[32,2048]{1,0:T(8,128)(2,1)S(1)}, bf16[32,2048]{1,0:T(8,128)(2,1)S(1)}, u32[]{:S(2)}, u32[]{:S(2)}) %collective-permute-start.4) | collective-permute-done | bytes 131104 | tf_op jit(solution)/shard_map/ppermute | solution.py:39
  95.4 0.2 collective-permute-done.6
  95.6 1.5 collective-permute-start.7
  97.1 1.5 collective-permute-done.7
  98.6 23.0 %all-gather.3.cloned.1.call-done = bf16[6144,704]{1,0:T(8,128)(2,1)} async-done(((bf16[192,704]{1,0:T(8,128)(2,1)}), bf16[6144,704]{1,0:T(8,128)(2,1)}) %all-gather.3.cloned.1.call-update) | async-done | bytes 8650768 | tf_op jit(solution)/shard_map/all_gather | solution.py:334
  121.6 9.6 %feed_forward.1 = (f32[128,2048]{1,0:T(8,128)}, bf16[128,2048]{1,0:T(8,128)(2,1)}) custom-call(bf16[256,2048]{1,0:T(8,128)(2,1)} %copy-done.2, bf16[32,192,704]{2,1,0:T(8,128)(2,1)} %bitcast.48, bf16[32,192,704]{2,1,0:T(8,128)(2,1)} %bitcast.49, bf16[32,192,704]{2,1,0:T(8,128)(2,1)} %bitcast.50), custom_call_target="tpu_custom_call" | custom-call | tf_op jit(solution)/shard_map/feed_forward/pallas_call | solution.py:271
  131.2 1.4 collective-permute-start.8
  132.6 1.7 %collective-permute-done.8 = bf16[128,2048]{1,0:T(8,128)(2,1)S(1)} collective-permute-done((bf16[128,2048]{1,0:T(8,128)(2,1)}, bf16[128,2048]{1,0:T(8,128)(2,1)S(1)}, u32[]{:S(2)}, u32[]{:S(2)}) %collective-permute-start.8) | collective-permute-done | bytes 524320 | tf_op jit(solution)/shard_map/ppermute | solution.py:39
  134.3 1.4 fusion.12
  135.7 2.8 %collective-permute-start.10 = (bf16[32,2048]{1,0:T(8,128)(2,1)S(1)}, bf16[32,2048]{1,0:T(8,128)(2,1)S(1)}, u32[]{:S(2)}, u32[]{:S(2)}) collective-permute-start(bf16[32,2048]{1,0:T(8,128)(2,1)S(1)} %get-tuple-element.27), channel_id=1, source_target_pairs={{0,4},{2,6},{4,0},{6,2},{1,5},{3,7},{5,1},{7,3},{8,12},{10,14},{12... | collective-permute-start | bytes 393224 | tf_op jit(solution)/shard_map/ppermute | solution.py:39
  138.5 0.3 collective-permute-start.11
  138.8 2.4 %collective-permute-start.9 = (bf16[32,2048]{1,0:T(8,128)(2,1)S(1)}, bf16[32,2048]{1,0:T(8,128)(2,1)S(1)}, u32[]{:S(2)}, u32[]{:S(2)}) collective-permute-start(bf16[32,2048]{1,0:T(8,128)(2,1)S(1)} %get-tuple-element.25), channel_id=1, source_target_pairs={{0,6},{2,0},{4,2},{6,4},{1,7},{3,1},{5,3},{7,5},{8,14},{10,8},{12,... | collective-permute-start | bytes 393224 | tf_op jit(solution)/shard_map/ppermute | solution.py:39
  141.2 0.8 collective-permute-done.10
  142.0 3.3 %collective-permute-done.11 = bf16[32,2048]{1,0:T(8,128)(2,1)S(1)} collective-permute-done((bf16[32,2048]{1,0:T(8,128)(2,1)S(1)}, bf16[32,2048]{1,0:T(8,128)(2,1)S(1)}, u32[]{:S(2)}, u32[]{:S(2)}) %collective-permute-start.11) | collective-permute-done | bytes 131104 | tf_op jit(solution)/shard_map/ppermute | solution.py:39
  145.3 0.7 fusion.6
  (37 shorter events, 0.4 us)
Async XLA Ops:
  6.5 61.6 %copy-start = (bf16[128,2048]{1,0:T(8,128)(2,1)S(1)}, bf16[128,2048]{1,0:T(8,128)(2,1)}, u32[]{:S(2)}) copy-start(bf16[128,2048]{1,0:T(8,128)(2,1)} %param.29) | copy-start | bytes 1572868
  6.5 115.1 %all-gather.3.cloned.1.call-start = ((), (), s32[]{:S(2)}) async-start(), calls=%async_computation.1 | async-start | bytes 9732096 | tf_op jit(solution)/shard_map/all_gather | solution.py:334
  11.1 0.9 copy-start.6
  11.1 2.9 %copy-start.8 = (f32[8,256]{1,0:T(8,128)S(1)}, f32[8,256]{1,0:T(8,128)}, u32[]{:S(2)}) copy-start(f32[8,256]{1,0:T(8,128)} %param.28) | copy-start | bytes 24580
  17.3 21.1 %copy-start.3 = (f32[2,8,16,64]{3,2,1,0:T(8,128)S(1)}, f32[2,8,16,64]{3,2,1,0:T(8,128)}, u32[]{:S(2)}) copy-start(f32[2,8,16,64]{3,2,1,0:T(8,128)} %param.26) | copy-start | bytes 196612
  17.3 21.2 %copy-start.4 = (f32[2,8,16,64]{3,2,1,0:T(8,128)S(1)}, f32[2,8,16,64]{3,2,1,0:T(8,128)}, u32[]{:S(2)}) copy-start(f32[2,8,16,64]{3,2,1,0:T(8,128)} %param.25) | copy-start | bytes 196612
  26.3 32.9 %all-to-all-start = ((f32[32,4,8,128]{3,2,1,0:T(8,128)}), f32[32,4,8,128]{3,2,1,0:T(8,128)S(1)}, u32[]{:S(2)}, u32[]{:S(2)}) async-start(f32[32,4,8,128]{3,2,1,0:T(8,128)} %broadcast_in_dim.16), calls=%async_computation | async-start | bytes 1048576 | tf_op jit(solution)/shard_map/all_to_all | solution.py:367
  59.2 0.8 copy-start.1
  69.4 16.3 %copy-start.5 = (bf16[32,2048]{1,0:T(8,128)(2,1)S(1)}, bf16[32,2048]{1,0:T(8,128)(2,1)}, u32[]{:S(2)}) copy-start(bf16[32,2048]{1,0:T(8,128)(2,1)} %param.18) | copy-start | bytes 393220
  69.4 16.5 %copy-start.7 = (f32[2048]{0:T(1024)S(1)}, f32[2048]{0:T(1024)}, u32[]{:S(2)}) copy-start(f32[2048]{0:T(1024)} %param.30) | copy-start | bytes 24580
  69.5 3.8 %collective-permute-start = (bf16[128,2048]{1,0:T(8,128)(2,1)S(1)}, bf16[128,2048]{1,0:T(8,128)(2,1)S(1)}, u32[]{:S(2)}, u32[]{:S(2)}) collective-permute-start(bf16[128,2048]{1,0:T(8,128)(2,1)S(1)} %slice.133), channel_id=1, source_target_pairs={{0,1},{1,0},{2,3},{3,2},{4,5},{5,4},{6,7},{7,6},{8,9},{9,8},{10,11... | collective-permute-start | bytes 1572872 | tf_op jit(solution)/shard_map/ppermute | solution.py:39
  73.4 5.6 %collective-permute-start.1 = (bf16[32,2048]{1,0:T(8,128)(2,1)S(1)}, bf16[32,2048]{1,0:T(8,128)(2,1)S(1)}, u32[]{:S(2)}, u32[]{:S(2)}) collective-permute-start(bf16[32,2048]{1,0:T(8,128)(2,1)S(1)} %get-tuple-element.28), channel_id=1, source_target_pairs={{0,6},{2,0},{4,2},{6,4},{1,7},{3,1},{5,3},{7,5},{8,14},{10,8},{12,... | collective-permute-start | bytes 393224 | tf_op jit(solution)/shard_map/ppermute | solution.py:39
  75.9 5.9 %collective-permute-start.2 = (bf16[32,2048]{1,0:T(8,128)(2,1)S(1)}, bf16[32,2048]{1,0:T(8,128)(2,1)S(1)}, u32[]{:S(2)}, u32[]{:S(2)}) collective-permute-start(bf16[32,2048]{1,0:T(8,128)(2,1)S(1)} %get-tuple-element.30), channel_id=1, source_target_pairs={{0,4},{2,6},{4,0},{6,2},{1,5},{3,7},{5,1},{7,3},{8,12},{10,14},{12... | collective-permute-start | bytes 393224 | tf_op jit(solution)/shard_map/ppermute | solution.py:39
  76.4 9.3 %collective-permute-start.3 = (bf16[32,2048]{1,0:T(8,128)(2,1)S(1)}, bf16[32,2048]{1,0:T(8,128)(2,1)S(1)}, u32[]{:S(2)}, u32[]{:S(2)}) collective-permute-start(bf16[32,2048]{1,0:T(8,128)(2,1)S(1)} %get-tuple-element.29), channel_id=1, source_target_pairs={{0,2},{2,4},{4,6},{6,0},{1,3},{3,5},{5,7},{7,1},{8,10},{10,12},{12... | collective-permute-start | bytes 393224 | tf_op jit(solution)/shard_map/ppermute | solution.py:39
  86.1 9.3 %collective-permute-start.4 = (bf16[32,2048]{1,0:T(8,128)(2,1)S(1)}, bf16[32,2048]{1,0:T(8,128)(2,1)S(1)}, u32[]{:S(2)}, u32[]{:S(2)}) collective-permute-start(bf16[32,2048]{1,0:T(8,128)(2,1)S(1)} %get-tuple-element.20), channel_id=1, source_target_pairs={{0,2},{2,4},{4,6},{6,0},{1,3},{3,5},{5,7},{7,1},{8,10},{10,12},{12... | collective-permute-start | bytes 393224 | tf_op jit(solution)/shard_map/ppermute | solution.py:39
  86.3 9.0 %collective-permute-start.5 = (bf16[32,2048]{1,0:T(8,128)(2,1)S(1)}, bf16[32,2048]{1,0:T(8,128)(2,1)S(1)}, u32[]{:S(2)}, u32[]{:S(2)}) collective-permute-start(bf16[32,2048]{1,0:T(8,128)(2,1)S(1)} %get-tuple-element.20), channel_id=1, source_target_pairs={{0,4},{2,6},{4,0},{6,2},{1,5},{3,7},{5,1},{7,3},{8,12},{10,14},{12... | collective-permute-start | bytes 393224 | tf_op jit(solution)/shard_map/ppermute | solution.py:39
  86.8 8.7 %collective-permute-start.6 = (bf16[32,2048]{1,0:T(8,128)(2,1)S(1)}, bf16[32,2048]{1,0:T(8,128)(2,1)S(1)}, u32[]{:S(2)}, u32[]{:S(2)}) collective-permute-start(bf16[32,2048]{1,0:T(8,128)(2,1)S(1)} %get-tuple-element.20), channel_id=1, source_target_pairs={{0,6},{2,0},{4,2},{6,4},{1,7},{3,1},{5,3},{7,5},{8,14},{10,8},{12,... | collective-permute-start | bytes 393224 | tf_op jit(solution)/shard_map/ppermute | solution.py:39
  95.6 3.0 %collective-permute-start.7 = (bf16[128,2048]{1,0:T(8,128)(2,1)S(1)}, bf16[128,2048]{1,0:T(8,128)(2,1)S(1)}, u32[]{:S(2)}, u32[]{:S(2)}) collective-permute-start(bf16[128,2048]{1,0:T(8,128)(2,1)S(1)} %pad_maximum_fusion.1), channel_id=1, source_target_pairs={{0,1},{1,0},{2,3},{3,2},{4,5},{5,4},{6,7},{7,6},{8,9},{9,8},{10,11... | collective-permute-start | bytes 1572872 | tf_op jit(solution)/shard_map/ppermute | solution.py:39
  98.6 23.0 %copy-start.2 = (bf16[256,2048]{1,0:T(8,128)(2,1)}, bf16[256,2048]{1,0:T(8,128)(2,1)S(1)}, u32[]{:S(2)}) copy-start(bf16[256,2048]{1,0:T(8,128)(2,1)S(1)} %constant_dynamic-update-slice_fusion.rows_ref) | copy-start | bytes 3145732
  131.2 3.1 %collective-permute-start.8 = (bf16[128,2048]{1,0:T(8,128)(2,1)}, bf16[128,2048]{1,0:T(8,128)(2,1)S(1)}, u32[]{:S(2)}, u32[]{:S(2)}) collective-permute-start(bf16[128,2048]{1,0:T(8,128)(2,1)} %get-tuple-element.16), channel_id=1, source_target_pairs={{0,1},{1,0},{2,3},{3,2},{4,5},{5,4},{6,7},{7,6},{8,9},{9,8},{10,11... | collective-permute-start | bytes 1572872 | tf_op jit(solution)/shard_map/ppermute | solution.py:39
  135.7 6.3 %collective-permute-start.10 = (bf16[32,2048]{1,0:T(8,128)(2,1)S(1)}, bf16[32,2048]{1,0:T(8,128)(2,1)S(1)}, u32[]{:S(2)}, u32[]{:S(2)}) collective-permute-start(bf16[32,2048]{1,0:T(8,128)(2,1)S(1)} %get-tuple-element.27), channel_id=1, source_target_pairs={{0,4},{2,6},{4,0},{6,2},{1,5},{3,7},{5,1},{7,3},{8,12},{10,14},{12... | collective-permute-start | bytes 393224 | tf_op jit(solution)/shard_map/ppermute | solution.py:39
  138.5 6.8 %collective-permute-start.11 = (bf16[32,2048]{1,0:T(8,128)(2,1)S(1)}, bf16[32,2048]{1,0:T(8,128)(2,1)S(1)}, u32[]{:S(2)}, u32[]{:S(2)}) collective-permute-start(bf16[32,2048]{1,0:T(8,128)(2,1)S(1)} %get-tuple-element.26), channel_id=1, source_target_pairs={{0,2},{2,4},{4,6},{6,0},{1,3},{3,5},{5,7},{7,1},{8,10},{10,12},{12... | collective-permute-start | bytes 393224 | tf_op jit(solution)/shard_map/ppermute | solution.py:39
  138.8 6.5 %collective-permute-start.9 = (bf16[32,2048]{1,0:T(8,128)(2,1)S(1)}, bf16[32,2048]{1,0:T(8,128)(2,1)S(1)}, u32[]{:S(2)}, u32[]{:S(2)}) collective-permute-start(bf16[32,2048]{1,0:T(8,128)(2,1)S(1)} %get-tuple-element.25), channel_id=1, source_target_pairs={{0,6},{2,0},{4,2},{6,4},{1,7},{3,1},{5,3},{7,5},{8,14},{10,8},{12,... | collective-permute-start | bytes 393224 | tf_op jit(solution)/shard_map/ppermute | solution.py:39
Sparse Core Ops, SparseCore 0:
  9.9 111.6 all-gather.2

commit v2 on v1

v2 whole, which is shorter than its diff:
```python
import jax
import jax.numpy as jnp
from jax import lax
from jax.experimental import pallas as pl
from jax.experimental.pallas import tpu as pltpu
from jax.sharding import Mesh
from jax.sharding import PartitionSpec as P


GROUP = 16
COST = 2_000_000_000
SP = ("z", "y")
TP = ("x", "c")
HIGHEST = lax.Precision.HIGHEST


def discretize(log_dt, decay_rate, frequency):
    step_size = jnp.exp(log_dt)
    magnitude = jnp.exp(-step_size * decay_rate)
    angle_step = step_size * frequency
    state_real = magnitude * jnp.cos(angle_step)
    state_imag = magnitude * jnp.sin(angle_step)
    denominator = decay_rate * decay_rate + frequency * frequency
    shifted = state_real - 1.0
    zoh_real = (-shifted * decay_rate + state_imag * frequency) / denominator
    zoh_imag = (-state_imag * decay_rate - shifted * frequency) / denominator
    return (state_real, state_imag, zoh_real, zoh_imag)


def on_ring(array, axis, shift):
    size = lax.axis_size(axis)
    return lax.ppermute(array, axis, [(i, (i + shift) % size) for i in range(size)])


def flip_matrix(count, dtype):
    rows = lax.broadcasted_iota(jnp.int32, (count, count), 0)
    cols = lax.broadcasted_iota(jnp.int32, (count, count), 1)
    return jnp.where(rows + cols == count - 1, 1.0, 0.0).astype(dtype)


def times_transposed(left, right, precision=None):
    return lax.dot_general(
        left,
        right,
        (((1,), (1,)), ((), ())),
        precision=precision,
        preferred_element_type=jnp.float32,
    )


def side_by_side(left, right):
    return jnp.concatenate([left, right], axis=1)


def local_states_kernel(
    u_ref,
    keep_ref,
    docs_ref,
    dt_ref,
    rates_ref,
    freq_ref,
    map_real_ref,
    map_imag_ref,
    real_ref,
    imag_ref,
    decay_ref,
    pole_ref,
    summary_ref,
    drive_ref,
):
    tokens, channels = u_ref.shape
    groups, lanes = pole_ref.shape[1:]
    diagonal = lax.broadcasted_iota(jnp.int32, (groups, groups), 0) == lax.broadcasted_iota(
        jnp.int32, (groups, groups), 1
    )
    log_dt = jnp.sum(jnp.where(diagonal, dt_ref[...], 0.0), axis=1, keepdims=True)
    state_real, state_imag, zoh_real, zoh_imag = discretize(
        log_dt, side_by_side(rates_ref[...], rates_ref[...]), side_by_side(freq_ref[...], freq_ref[...])
    )
    pole_ref[0] = state_real
    pole_ref[1] = state_imag
    docs = docs_ref[...].astype(jnp.float32)
    place = lax.broadcasted_iota(jnp.int32, docs.shape, 1)
    from_left = (docs == pltpu.roll(docs, 1, 1)) | (place == 0)
    from_right = (docs == pltpu.roll(docs, tokens - 1, 1)) | (place == tokens - 1)
    keep = jnp.exp(keep_ref[...])
    factors = jnp.concatenate(
        [jnp.where(from_left, keep, 0.0), jnp.where(from_right, keep, 0.0)], axis=0
    )
    flip = flip_matrix(tokens, jnp.float32)
    rows = lax.broadcasted_iota(jnp.int32, (tokens, tokens), 0)
    cols = lax.broadcasted_iota(jnp.int32, (tokens, tokens), 1)
    same = jnp.where(rows == cols, 1.0, 0.0)
    ahead_factor = times_transposed(same, factors, HIGHEST)
    back_factor = times_transposed(flip, factors, HIGHEST)
    u = u_ref[...]
    backward = jnp.dot(
        flip.astype(jnp.bfloat16), u, preferred_element_type=jnp.float32
    ).astype(jnp.bfloat16)
    both = jnp.concatenate([u, backward], axis=1)
    ahead = lax.broadcasted_iota(jnp.int32, (tokens, lanes), 1) < lanes // 2
    part = ahead[:GROUP]
    drive_ref[...] = jnp.zeros(drive_ref.shape, jnp.float32)
    for g in range(groups):
        scale_real, scale_imag = (zoh_real[g : g + 1], zoh_imag[g : g + 1])
        in_real, in_imag = (
            side_by_side(ref[0, g], ref[1, g]) for ref in (map_real_ref, map_imag_ref)
        )
        map_real = scale_real * in_real - scale_imag * in_imag
        map_imag = scale_real * in_imag + scale_imag * in_real
        at = g * GROUP
        drive_ref[at : at + GROUP, :lanes] = jnp.where(part, map_real, 0.0)
        drive_ref[at : at + GROUP, lanes:] = jnp.where(part, map_imag, 0.0)
        drive_ref[channels + at : channels + at + GROUP, :lanes] = jnp.where(part, 0.0, map_real)
        drive_ref[channels + at : channels + at + GROUP, lanes:] = jnp.where(part, 0.0, map_imag)
        whole = drive_ref[...]
        drive_ref[at : at + GROUP] = jnp.zeros((GROUP, 2 * lanes), jnp.float32)
        drive_ref[channels + at : channels + at + GROUP] = jnp.zeros(
            (GROUP, 2 * lanes), jnp.float32
        )
        first = whole.astype(jnp.bfloat16)
        rest = whole - first.astype(jnp.float32)
        second = rest.astype(jnp.bfloat16)
        third = (rest - second.astype(jnp.float32)).astype(jnp.bfloat16)
        drive = jnp.dot(both, first, preferred_element_type=jnp.float32)
        drive = drive + jnp.dot(both, second, preferred_element_type=jnp.float32)
        drive = drive + jnp.dot(both, third, preferred_element_type=jnp.float32)
        real_ref[:, g, :] = drive[:, :lanes]
        imag_ref[:, g, :] = drive[:, lanes:]
        decay_ref[:, g, :] = jnp.where(
            ahead, ahead_factor[:, g : g + 1], back_factor[:, groups + g : groups + g + 1]
        )
    pole_real, pole_imag = (pole_ref[0], pole_ref[1])

    def step(t, carry):
        state_real, state_imag, product = carry
        factor = decay_ref[t]
        step_real, step_imag = (factor * pole_real, factor * pole_imag)
        return (
            step_real * state_real - step_imag * state_imag + real_ref[t],
            step_real * state_imag + step_imag * state_real + imag_ref[t],
            product * factor,
        )

    zero = jnp.zeros((groups, lanes), jnp.float32)
    state_real, state_imag, product = lax.fori_loop(
        0, tokens, step, (zero, zero, zero + 1.0), unroll=8
    )
    summary_ref[0] = state_real
    summary_ref[1] = state_imag
    summary_ref[2] = product
    first_doc, last_doc = (
        jnp.broadcast_to(docs[:, :1], (groups, lanes)),
        jnp.broadcast_to(docs[:, tokens - 1 :], (groups, lanes)),
    )
    summary_ref[3] = jnp.where(
        ahead[:groups], 8.0 * first_doc + last_doc, 8.0 * last_doc + first_doc
    )


def near_of(code):
    return jnp.floor(code * 0.125)


def squared(real, imag, times):
    for _ in range(times):
        real, imag = (real * real - imag * imag, 2.0 * real * imag)
    return (real, imag)


def pick(ref, ahead, j, last):
    return tuple(jnp.where(ahead, ref[j, k], ref[last - j, k]) for k in range(4))


def row_kernel(place_ref, own_ref, *refs):
    arrived, pole_ref, row_ref, group_ref = (refs[:3], refs[3], refs[4], refs[5])
    groups, lanes = pole_ref.shape[1:]
    row_ref[place_ref[1]] = own_ref[...]
    for back, ref in zip((1, 3, 2), arrived):
        row_ref[(place_ref[1] + 4 - back) % 4] = ref[...]
    ahead = lax.broadcasted_iota(jnp.int32, (groups, lanes), 1) < lanes // 2
    far_real, far_imag = squared(pole_ref[0], pole_ref[1], 8)
    state_real, state_imag, product, code = pick(row_ref, ahead, 0, 3)
    first = near_of(code)
    last = code - 8.0 * first
    for j in range(1, 4):
        local_real, local_imag, factor, code = pick(row_ref, ahead, j, 3)
        near = near_of(code)
        kept = jnp.where(near == last, factor, 0.0)
        last = code - 8.0 * near
        state_real, state_imag = (
            kept * (far_real * state_real - far_imag * state_imag) + local_real,
            kept * (far_real * state_imag + far_imag * state_real) + local_imag,
        )
        product = product * kept
    group_ref[0] = state_real
    group_ref[1] = state_imag
    group_ref[2] = product
    group_ref[3] = 8.0 * first + last


def mixing_kernel(
    place_ref,
    row_ref,
    *refs,
):
    group_refs = refs[:8]
    (
        u_ref,
        real_ref,
        imag_ref,
        decay_ref,
        pole_ref,
        read_real_ref,
        read_imag_ref,
        skip_ref,
        out_ref,
        all_ref,
        state_real_ref,
        state_imag_ref,
        mixed_ref,
        matrix_ref,
    ) = refs[8:]
    tokens, channels = u_ref.shape
    groups, lanes = pole_ref.shape[1:]
    pole_real, pole_imag = (pole_ref[0], pole_ref[1])
    for back, ref in enumerate(group_refs):
        all_ref[(place_ref[0] + 8 - back) % 8] = ref[...]
    ahead = lax.broadcasted_iota(jnp.int32, (groups, lanes), 1) < lanes // 2
    zero = jnp.zeros((groups, lanes), jnp.float32)
    state = (zero, zero, zero - 1.0)
    for ref, here, blocks, far in (
        (all_ref, place_ref[0], 8, squared(pole_real, pole_imag, 10)),
        (row_ref, place_ref[1], 4, squared(pole_real, pole_imag, 8)),
    ):
        for j in range(blocks - 1):
            state_real, state_imag, last = state
            local_real, local_imag, product, code = pick(ref, ahead, j, blocks - 1)
            ours = jnp.where(j < here, 1, 0)
            theirs = jnp.where(blocks - 1 - j > here, 1, 0)
            before = jnp.where(ahead, ours, theirs) > 0
            near = near_of(code)
            kept = jnp.where(near == last, product, 0.0)
            next_real = kept * (far[0] * state_real - far[1] * state_imag) + local_real
            next_imag = kept * (far[0] * state_imag + far[1] * state_real) + local_imag
            state = (
                jnp.where(before, next_real, state_real),
                jnp.where(before, next_imag, state_imag),
                jnp.where(before, code - 8.0 * near, last),
            )
    joined = near_of(row_ref[place_ref[1], 3]) == state[2]
    enter_real = jnp.where(joined, state[0], 0.0)
    enter_imag = jnp.where(joined, state[1], 0.0)

    def step(t, carry):
        state_real, state_imag = carry
        factor = decay_ref[t]
        step_real, step_imag = (factor * pole_real, factor * pole_imag)
        next_real = step_real * state_real - step_imag * state_imag + real_ref[t]
        next_imag = step_real * state_imag + step_imag * state_real + imag_ref[t]
        state_real_ref[t] = next_real
        state_imag_ref[t] = next_imag
        return (next_real, next_imag)

    lax.fori_loop(0, tokens, step, (enter_real, enter_imag), unroll=8)
    read = jnp.zeros((tokens, 2 * channels), jnp.float32)
    matrix_ref[...] = jnp.zeros(matrix_ref.shape, jnp.float32)
    part = lax.broadcasted_iota(jnp.int32, (GROUP, lanes), 1) < lanes // 2
    for g in range(groups):
        states = jnp.concatenate([state_real_ref[:, g, :], state_imag_ref[:, g, :]], axis=1)
        out_real = side_by_side(read_real_ref[0, g], read_real_ref[1, g])
        out_imag = -side_by_side(read_imag_ref[0, g], read_imag_ref[1, g])
        at = g * GROUP
        matrix_ref[at : at + GROUP, :lanes] = jnp.where(part, out_real, 0.0)
        matrix_ref[at : at + GROUP, lanes:] = jnp.where(part, out_imag, 0.0)
        matrix_ref[channels + at : channels + at + GROUP, :lanes] = jnp.where(part, 0.0, out_real)
        matrix_ref[channels + at : channels + at + GROUP, lanes:] = jnp.where(part, 0.0, out_imag)
        read = read + times_transposed(states, matrix_ref[...], HIGHEST)
        matrix_ref[at : at + GROUP] = jnp.zeros((GROUP, 2 * lanes), jnp.float32)
        matrix_ref[channels + at : channels + at + GROUP] = jnp.zeros(
            (GROUP, 2 * lanes), jnp.float32
        )
    backward = jnp.dot(
        flip_matrix(tokens, jnp.float32),
        read[:, channels:],
        precision=HIGHEST,
        preferred_element_type=jnp.float32,
    )
    pre = read[:, :channels] + backward + skip_ref[...] * u_ref[...].astype(jnp.float32)
    mixed_ref[...] = jax.nn.gelu(pre)
    rows = tokens // 8
    for k in range(8):
        start = pl.multiple_of(place_ref[2 + k] * rows, rows)
        out_ref[k * rows : (k + 1) * rows, :] = mixed_ref[pl.ds(start, rows), :].astype(
            jnp.bfloat16
        )


def feed_forward_kernel(
    place_ref,
    rows_ref,
    own_ref,
    low_left_ref,
    high_left_ref,
    low_right_ref,
    high_right_ref,
    low_far_ref,
    high_far_ref,
    down_ref,
    keep_ref,
    send_ref,
    gate_to,
    up_to,
    down_to,
    sems,
):
    depth, hidden = down_to.shape[2:]
    half = low_far_ref.shape[0]
    column = [(place_ref[1] + 4 - back) % 4 for back in (0, 1, 3, 2)]
    copies = ([], [], [])
    for which, target in enumerate((gate_to, up_to)):
        span = pl.ds(which * depth, depth)
        for source, dest in (
            (own_ref, target.at[:, column[0]]),
            (low_left_ref, target.at[:half, column[1]]),
            (high_left_ref, target.at[half:, column[1]]),
            (low_right_ref, target.at[:half, column[2]]),
            (high_right_ref, target.at[half:, column[2]]),
            (low_far_ref, target.at[:half, column[3]]),
            (high_far_ref, target.at[half:, column[3]]),
        ):
            copies[which].append(pltpu.make_async_copy(source.at[:, span], dest, sems.at[which]))
    for m in range(4):
        copies[2].append(
            pltpu.make_async_copy(
                down_ref.at[:, pl.ds(m * depth, depth)], down_to.at[:, column[m]], sems.at[2]
            )
        )
    for group in copies:
        for copy in group:
            copy.start()
    rows = rows_ref[...]
    features = rows.shape[1]
    for copy in copies[0]:
        copy.wait()
    gate = jnp.dot(
        rows, gate_to[...].reshape(features, hidden), preferred_element_type=jnp.float32
    )
    for copy in copies[1]:
        copy.wait()
    up = jnp.dot(rows, up_to[...].reshape(features, hidden), preferred_element_type=jnp.float32)
    inner = (gate / (1.0 + jnp.exp(-gate)) * up).astype(jnp.bfloat16)
    for copy in copies[2]:
        copy.wait()
    near = keep_ref.shape[0]
    count = 2
    width = count * 4 * depth
    for z in range(0, down_to.shape[0], count):
        made = times_transposed(inner, down_to[z : z + count].reshape(width, hidden))
        at = z * 4 * depth
        keep_ref[:, at : at + width] = made[:near]
        send_ref[:, at : at + width] = made[near:].astype(jnp.bfloat16)


def feed_forward(place, rows, pieces):
    tokens, features = rows.shape
    hidden = pieces[0].shape[2]
    scratch = pltpu.VMEM((8, 4, features // 32, hidden), jnp.bfloat16)
    return pl.pallas_call(
        feed_forward_kernel,
        in_specs=[IN_SMEM, IN_VMEM] + [pl.BlockSpec(memory_space=pl.ANY)] * len(pieces),
        out_shape=[
            jax.ShapeDtypeStruct((tokens // 2, features), jnp.float32),
            jax.ShapeDtypeStruct((tokens // 2, features), jnp.bfloat16),
        ],
        scratch_shapes=[scratch, scratch, scratch, pltpu.SemaphoreType.DMA((3,))],
        name="feed_forward",
    )(place, rows, *pieces)


IN_VMEM = pl.BlockSpec(memory_space=pltpu.VMEM)
IN_SMEM = pl.BlockSpec(memory_space=pltpu.SMEM)


def summed_over_tp(keep, send):
    pair = keep + on_ring(send, "c", 1).astype(jnp.float32)
    chips = lax.axis_size("x")
    rows = pair.shape[0] // chips
    total = pair[:rows]
    away = pair.astype(jnp.bfloat16)
    for k in range(1, chips):
        arrived = on_ring(away[k * rows : (k + 1) * rows], "x", -k)
        total = total + arrived.astype(jnp.float32)
    return total


def local(
    mix_input,
    stream,
    doc_ids,
    log_dt,
    decay_rate,
    frequency,
    input_real,
    input_imag,
    output_real,
    output_imag,
    skip_gain,
    log_keep,
    proj_weight,
    norm_gain,
    gate_weight,
    up_weight,
    down_weight,
):
    chips = lax.axis_size("x")
    chip, core = (lax.axis_index("x"), lax.axis_index("c"))
    tokens, channels = mix_input.shape
    groups, states = decay_rate.shape
    lanes = 2 * states
    spare = -gate_weight.shape[1] % 128
    gate_up = jnp.pad(jnp.concatenate([gate_weight, up_weight], axis=0), ((0, 0), (0, spare)))
    own = lax.all_gather(gate_up, "z", axis=0, tiled=False)
    down = jnp.pad(down_weight.T, ((0, 0), (0, spare)))
    down_row = [on_ring(down, "y", k) for k in (1, -1, 2)]
    by_token = jax.ShapeDtypeStruct((tokens, groups, lanes), jnp.float32)
    drive_real, drive_imag, decays, poles, summary = pl.pallas_call(
        local_states_kernel,
        out_shape=[by_token] * 3
        + [jax.ShapeDtypeStruct((k, groups, lanes), jnp.float32) for k in (2, 4)],
        scratch_shapes=[pltpu.VMEM((2 * channels, 2 * lanes), jnp.float32)],
        name="local_states",
    )(
        mix_input,
        log_keep,
        doc_ids[None],
        log_dt[None],
        decay_rate,
        frequency,
        input_real.transpose(0, 1, 3, 2),
        input_imag.transpose(0, 1, 3, 2),
    )
    order = [
        2 * ((chip + chips - k) & (chips - 1)) + (core if same else 1 - core)
        for same in (True, False)
        for k in range(4)
    ]
    place = jnp.stack([lax.axis_index("z"), lax.axis_index("y"), *order]).astype(jnp.int32)
    summary, down_row = lax.optimization_barrier((summary, down_row))
    down_row = jnp.concatenate([down] + down_row, axis=0)
    down_all = lax.all_gather(down_row, "z", axis=0, tiled=False)
    row, group = pl.pallas_call(
        row_kernel,
        in_specs=[IN_SMEM] + [IN_VMEM] * 5,
        out_shape=[
            jax.ShapeDtypeStruct((4, *summary.shape), jnp.float32),
            jax.ShapeDtypeStruct(summary.shape, jnp.float32),
        ],
        name="row",
    )(place, summary, *(on_ring(summary, "y", k) for k in (1, -1, 2)), poles)
    found = [on_ring(group, "z", k) for k in range(1, 8)]
    found, own = lax.optimization_barrier((found, own))
    half = own.shape[0] // 2
    low, high = (own[:half], own[half:])
    low_left = on_ring(low, "y", 1)
    high_right = on_ring(high, "y", -1)
    high_left = on_ring(high, "y", 1)
    low_right = on_ring(low, "y", -1)
    mixed = pl.pallas_call(
        mixing_kernel,
        out_shape=jax.ShapeDtypeStruct((tokens, channels), jnp.bfloat16),
        in_specs=[IN_SMEM] + [IN_VMEM] * 17,
        scratch_shapes=[
            pltpu.VMEM((8, *summary.shape), jnp.float32),
            pltpu.VMEM((tokens, groups, lanes), jnp.float32),
            pltpu.VMEM((tokens, groups, lanes), jnp.float32),
            pltpu.VMEM((tokens, channels), jnp.float32),
            pltpu.VMEM((2 * channels, 2 * lanes), jnp.float32),
        ],
        name="mixing",
        cost_estimate=pl.CostEstimate(flops=COST, bytes_accessed=0, transcendentals=0),
    )(
        place,
        row,
        group,
        *found,
        mix_input,
        drive_real,
        drive_imag,
        decays,
        poles,
        output_real,
        output_imag,
        skip_gain[None],
    )
    product = jnp.dot(mixed, proj_weight, preferred_element_type=jnp.float32)
    branch = summed_over_tp(product[: tokens // 2], product[tokens // 2 :].astype(jnp.bfloat16))
    resid = stream.astype(jnp.float32) + branch
    scale = lax.rsqrt(jnp.mean(resid * resid, axis=-1, keepdims=True) + 1e-06)
    normed = (resid * scale * norm_gain).astype(jnp.bfloat16)
    normed, low_left, high_right = lax.optimization_barrier((normed, low_left, high_right))
    far = (on_ring(low_left, "y", 1), on_ring(high_right, "y", -1))
    mine = jnp.concatenate([normed] + [on_ring(normed, "x", k) for k in range(1, chips)], axis=0)
    rows = jnp.concatenate([mine, on_ring(mine, "c", 1)], axis=0)
    ffn = summed_over_tp(*feed_forward(
        place, rows, (own, low_left, high_left, low_right, high_right, *far, down_all)
    ))
    return (resid + 0.5 * ffn).astype(jnp.bfloat16)


def solution(mesh):
    torus = Mesh(mesh.devices.reshape(8, 4, 4, 2), ("z", "y", "x", "c"))
    everything = SP + TP
    in_specs = (
        P(SP, TP),
        P(everything, None),
        P(SP),
        P(TP),
        P(TP, None),
        P(TP, None),
        P(None, TP, None, None),
        P(None, TP, None, None),
        P(None, TP, None, None),
        P(None, TP, None, None),
        P(TP),
        P(TP, SP),
        P(TP, None),
        P(),
        P(SP, TP),
        P(SP, TP),
        P(TP, SP),
    )

    return jax.shard_map(
        local, mesh=torus, in_specs=in_specs, out_specs=P(everything, None), check_vma=False
    )
```

time: 153 us -> 163 us (1.065)
  starting transfers between devices: 29.1 us -> 52.6 us
  other arithmetic: 11.3 us -> 5.11 us
  local copies, waits for them, and re-layouts: 6.4 us -> 3.96 us
  Pallas kernels: 24.5 us -> 22.8 us
  waiting for transfers between devices: 65.3 us -> 63.6 us
    ppermute x12 -> x31, waiting for transfers between devices: 24.1 us -> 63.6 us  [on_ring(): lax.ppermute(array, axis, [(i, (i + shift) % size) for i in range(size)])]
    ppermute x12 -> x31, starting transfers between devices: 17.1 us -> 52.6 us  [on_ring(): lax.ppermute(array, axis, [(i, (i + shift) % size) for i in range(size)])]
    all_gather x1 -> x2, waiting for transfers between devices: 23 us -> 0.01 us  [the longest x1 0.01 us: local(): own = lax.all_gather(gate_up, 'z', axis=0, tiled=False)]
    all_to_all x1 -> x0, waiting for transfers between devices: 18.2 us -> none  [local(): lax.all_to_all(jnp.broadcast_to(summary, (blocks, *summary.shape)), SP, s...]
    all_to_all x1 -> x0, starting transfers between devices: 12 us -> none  [local(): lax.all_to_all(jnp.broadcast_to(summary, (blocks, *summary.shape)), SP, s...]
    concatenate x7 -> x3, other arithmetic: 5.14 us -> 2.55 us  [the longest x1 1.71 us: local(): jnp.concatenate([gate_weight, up_weight], axis=0)]
    pallas_call x1 -> x2, Pallas kernels: 9.57 us -> 9.19 us  [the longest x1 7.75 us: feed_forward(): pl.pallas_call(feed_forward_kernel, in_specs=[IN_SMEM, IN_VMEM] + [pl.Blo...]
  transfers between devices with their start and end apart: 14 -> 33, of which waited for: 12 -> 18; matrix products, arithmetic and copies ran while one was open for 9% -> 3% of each run, Pallas kernels for 10% -> 9%
where the time goes in v2:
time: 163 us
  waiting for transfers between devices  63.6 us (39%)
  starting transfers between devices  52.6 us (32%)
  Pallas kernels  22.8 us (14%)
  between operations  13.7 us (8%)
  other arithmetic  5.11 us (3%)
  local copies, waits for them, and re-layouts  3.96 us (2%)
    ppermute x31, waiting for transfers between devices, on_ring(): lax.ppermute(array, axis, [(i, (i + shift) % size) for i in range(size)])  63.6 us
    ppermute x31, starting transfers between devices, on_ring(): lax.ppermute(array, axis, [(i, (i + shift) % size) for i in range(size)])  52.6 us
    pallas_call x1, Pallas kernels, feed_forward(): pl.pallas_call(feed_forward_kernel, in_specs=[IN_SMEM, IN_VMEM] + [pl.Blo...  7.75 us
    pallas_call x1, Pallas kernels, local(): pl.pallas_call(mixing_kernel, out_shape=jax.ShapeDtypeStruct((tokens, cha...  7 us
    pallas_call x1, Pallas kernels, local(): pl.pallas_call(local_states_kernel, out_shape=[by_token] * 3 + [jax.Shape...  6.56 us
  transfers between devices with their start and end apart: 33, of which 18 were waited for; matrix products, arithmetic and copies ran while one was open for 3% of the time, Pallas kernels for 9%

profile of v2, /device:TPU:1, one launch (start us, length us, event | category | flops | bytes accessed | tf_op | source)
XLA Modules:
  0.0 163.0 jit_solution(2897441333493463802)
XLA Ops:
  6.5 1.7 %fusion.10 = bf16[128,768]{1,0:T(8,128)(2,1)} fusion(bf16[64,704]{1,0:T(8,128)(2,1)} %param.32, bf16[64,704]{1,0:T(8,128)(2,1)} %param.31), kind=kLoop, calls=%fused_computation.20 | loop fusion | flops 688128 | bytes 376832 | tf_op jit(solution)/shard_map/concatenate | solution.py:422
  8.3 0.9 pad.8
  9.2 2.2 %collective-permute-start = (bf16[64,768]{1,0:T(8,128)(2,1)S(1)}, bf16[64,768]{1,0:T(8,128)(2,1)S(1)}, u32[]{:S(2)}, u32[]{:S(2)}) collective-permute-start(bf16[64,768]{1,0:T(8,128)(2,1)S(1)} %pad.8), channel_id=1, source_target_pairs={{0,8},{8,16},{16,24},{24,0},{1,9},{9,17},{17,25},{25,1},{2,10},{10... | collective-permute-start | bytes 294920 | tf_op jit(solution)/shard_map/ppermute | solution.py:32
  11.4 1.5 collective-permute-start.1
  13.0 1.6 collective-permute-start.2
  14.5 6.6 %local_states.1 = (f32[256,8,128]{2,1,0:T(8,128)}, f32[256,8,128]{2,1,0:T(8,128)}, f32[256,8,128]{2,1,0:T(8,128)}, f32[2,8,128]{2,1,0:T(8,128)}, f32[4,8,128]{2,1,0:T(8,128)}) custom-call(bf16[256,128]{1,0:T(8,128)(2,1)} %refs_8_.1, f32[8,256]{1,0:T(8,128)} %keep_ref.1, s32[1,256]{1,0:T(1,128)} %bitcast.26, f32[1,8]{1,0:T(1,128)} %bitcast.27, ...), custom_call_target="tpu_custom_call" | custom-call | tf_op jit(solution)/shard_map/local_states/pallas_call | solution.py:427
  21.1 0.8 pad_maximum_fusion.1
  21.9 0.5 collective-permute-start.3
  22.4 2.3 %collective-permute-start.4 = (f32[4,8,128]{2,1,0:T(8,128)}, f32[4,8,128]{2,1,0:T(8,128)S(1)}, u32[]{:S(2)}, u32[]{:S(2)}) collective-permute-start(f32[4,8,128]{2,1,0:T(8,128)} %get-tuple-element.30.own_ref), channel_id=1, source_target_pairs={{0,24},{8,0},{16,8},{24,16},{1,25},{9,1},{17,9},{25,17},{2,26},{10... | collective-permute-start | bytes 49160 | tf_op jit(solution)/shard_map/ppermute | solution.py:32
  24.7 0.2 collective-permute-start.5
  24.9 0.6 stack.43.place_ref
  25.5 0.5 collective-permute-done.3.refs_0_
  26.0 3.0 %collective-permute-done.5.refs_2_ = f32[4,8,128]{2,1,0:T(8,128)S(1)} collective-permute-done((f32[4,8,128]{2,1,0:T(8,128)}, f32[4,8,128]{2,1,0:T(8,128)S(1)}, u32[]{:S(2)}, u32[]{:S(2)}) %collective-permute-start.5) | collective-permute-done | bytes 16416 | tf_op jit(solution)/shard_map/ppermute | solution.py:32
  29.0 0.6 copy-done.11
  29.6 1.4 row.1
  31.1 6.4 %collective-permute-start.10 = (f32[4,8,128]{2,1,0:T(8,128)}, f32[4,8,128]{2,1,0:T(8,128)S(1)}, u32[]{:S(2)}, u32[]{:S(2)}) collective-permute-start(f32[4,8,128]{2,1,0:T(8,128)} %get-tuple-element.33.refs_0_), channel_id=1, source_target_pairs={{0,160},{32,192},{64,224},{96,0},{128,32},{160,64},{192,96},{224,1... | collective-permute-start | bytes 49160 | tf_op jit(solution)/shard_map/ppermute | solution.py:32
  37.5 0.3 collective-permute-start.11
  37.8 0.4 collective-permute-start.12
  38.2 1.2 collective-permute-start.6
  39.4 1.9 %collective-permute-start.7 = (f32[4,8,128]{2,1,0:T(8,128)}, f32[4,8,128]{2,1,0:T(8,128)S(1)}, u32[]{:S(2)}, u32[]{:S(2)}) collective-permute-start(f32[4,8,128]{2,1,0:T(8,128)} %get-tuple-element.33.refs_0_), channel_id=1, source_target_pairs={{0,64},{32,96},{64,128},{96,160},{128,192},{160,224},{192,0},{224,... | collective-permute-start | bytes 49160 | tf_op jit(solution)/shard_map/ppermute | solution.py:32
  41.3 2.2 %collective-permute-start.8 = (f32[4,8,128]{2,1,0:T(8,128)}, f32[4,8,128]{2,1,0:T(8,128)S(1)}, u32[]{:S(2)}, u32[]{:S(2)}) collective-permute-start(f32[4,8,128]{2,1,0:T(8,128)} %get-tuple-element.33.refs_0_), channel_id=1, source_target_pairs={{0,96},{32,128},{64,160},{96,192},{128,224},{160,0},{192,32},{224,... | collective-permute-start | bytes 49160 | tf_op jit(solution)/shard_map/ppermute | solution.py:32
  43.5 2.7 %collective-permute-start.9 = (f32[4,8,128]{2,1,0:T(8,128)}, f32[4,8,128]{2,1,0:T(8,128)S(1)}, u32[]{:S(2)}, u32[]{:S(2)}) collective-permute-start(f32[4,8,128]{2,1,0:T(8,128)} %get-tuple-element.33.refs_0_), channel_id=1, source_target_pairs={{0,128},{32,160},{64,192},{96,224},{128,0},{160,32},{192,64},{224,... | collective-permute-start | bytes 49160 | tf_op jit(solution)/shard_map/ppermute | solution.py:32
  46.3 0.8 collective-permute-done.8.refs_3_
  47.1 3.3 %collective-permute-done.9.refs_4_ = f32[4,8,128]{2,1,0:T(8,128)S(1)} collective-permute-done((f32[4,8,128]{2,1,0:T(8,128)}, f32[4,8,128]{2,1,0:T(8,128)S(1)}, u32[]{:S(2)}, u32[]{:S(2)}) %collective-permute-start.9) | collective-permute-done | bytes 16416 | tf_op jit(solution)/shard_map/ppermute | solution.py:32
  50.5 0.5 copy-done.19
  51.0 7.0 %mixing.1 = bf16[256,128]{1,0:T(8,128)(2,1)} custom-call(s32[10]{0:T(128)} %stack.43.place_ref, f32[4,4,8,128]{3,2,1,0:T(8,128)} %get-tuple-element.32.row_ref, f32[4,8,128]{2,1,0:T(8,128)} %get-tuple-element.33.refs_0_, f32[4,8,128]{2,1,0:T(8,128)} %copy-done.16, f32[4,8,128]{2,1,0:T(8,128)} %copy-done.17, f32[4,8,128]{2,1,0:T(8,128)} %copy-done.18, ...), custom_call_target="tpu_custom_call" | custom-call | flops 2000000000 | tf_op jit(solution)/shard_map/mixing/pallas_call | solution.py:469
  58.0 1.3 fusion.17
  59.3 5.6 %collective-permute-start.13 = (bf16[128,2048]{1,0:T(8,128)(2,1)S(1)}, bf16[128,2048]{1,0:T(8,128)(2,1)S(1)}, u32[]{:S(2)}, u32[]{:S(2)}) collective-permute-start(bf16[128,2048]{1,0:T(8,128)(2,1)S(1)} %slice.79), channel_id=1, source_target_pairs={{0,1},{1,0},{2,3},{3,2},{4,5},{5,4},{6,7},{7,6},{8,9},{9,8},{10,11... | collective-permute-start | bytes 1572872 | tf_op jit(solution)/shard_map/ppermute | solution.py:32
  65.0 1.5 collective-permute-done.13
  66.5 0.1 fusion.13
  66.7 2.6 %collective-permute-start.14 = (bf16[32,2048]{1,0:T(8,128)(2,1)S(1)}, bf16[32,2048]{1,0:T(8,128)(2,1)S(1)}, u32[]{:S(2)}, u32[]{:S(2)}) collective-permute-start(bf16[32,2048]{1,0:T(8,128)(2,1)S(1)} %get-tuple-element.64), channel_id=1, source_target_pairs={{0,6},{2,0},{4,2},{6,4},{1,7},{3,1},{5,3},{7,5},{8,14},{10,8},{12,... | collective-permute-start | bytes 393224 | tf_op jit(solution)/shard_map/ppermute | solution.py:32
  69.3 0.5 collective-permute-start.15
  69.8 0.6 collective-permute-start.16
  70.4 0.1 fusion.14
  70.6 1.5 collective-permute-start.23
  72.1 2.4 %collective-permute-done.14 = bf16[32,2048]{1,0:T(8,128)(2,1)S(1)} collective-permute-done((bf16[32,2048]{1,0:T(8,128)(2,1)S(1)}, bf16[32,2048]{1,0:T(8,128)(2,1)S(1)}, u32[]{:S(2)}, u32[]{:S(2)}) %collective-permute-start.14) | collective-permute-done | bytes 131104 | tf_op jit(solution)/shard_map/ppermute | solution.py:32
  74.4 0.7 collective-permute-done.15
  75.2 1.9 %collective-permute-start.24 = (bf16[4,128,768]{2,1,0:T(8,128)(2,1)S(1)}, bf16[4,128,768]{2,1,0:T(8,128)(2,1)S(1)}, u32[]{:S(2)}, u32[]{:S(2)}) collective-permute-start(bf16[4,128,768]{2,1,0:T(8,128)(2,1)S(1)} %get-tuple-element.60), channel_id=1, source_target_pairs={{0,24},{8,0},{16,8},{24,16},{1,25},{9,1},{17,9},{25,17},{2,26},{10... | collective-permute-start | bytes 2359304 | tf_op jit(solution)/shard_map/ppermute | solution.py:32
  77.1 2.0 %collective-permute-done.16 = bf16[32,2048]{1,0:T(8,128)(2,1)S(1)} collective-permute-done((bf16[32,2048]{1,0:T(8,128)(2,1)S(1)}, bf16[32,2048]{1,0:T(8,128)(2,1)S(1)}, u32[]{:S(2)}, u32[]{:S(2)}) %collective-permute-start.16) | collective-permute-done | bytes 131104 | tf_op jit(solution)/shard_map/ppermute | solution.py:32
  79.1 0.2 multiply_reduce_fusion
  79.3 0.1 multiply_convert_fusion
  79.4 27.2 %collective-permute-done.17.low_left_ref = bf16[4,128,768]{2,1,0:T(8,128)(2,1)S(1)} collective-permute-done((bf16[4,128,768]{2,1,0:T(8,128)(2,1)S(1)}, bf16[4,128,768]{2,1,0:T(8,128)(2,1)S(1)}, u32[]{:S(2)}, u32[]{:S(2)}) %collective-permute-start.17) | collective-permute-done | bytes 786464 | tf_op jit(solution)/shard_map/ppermute | solution.py:32
  106.6 1.6 collective-permute-start.19
  108.2 1.7 %collective-permute-start.20 = (bf16[32,2048]{1,0:T(8,128)(2,1)S(1)}, bf16[32,2048]{1,0:T(8,128)(2,1)S(1)}, u32[]{:S(2)}, u32[]{:S(2)}) collective-permute-start(bf16[32,2048]{1,0:T(8,128)(2,1)S(1)} %multiply_convert_fusion), channel_id=1, source_target_pairs={{0,4},{2,6},{4,0},{6,2},{1,5},{3,7},{5,1},{7,3},{8,12},{10,14},{12... | collective-permute-start | bytes 393224 | tf_op jit(solution)/shard_map/ppermute | solution.py:32
  110.0 0.9 collective-permute-start.21
  110.9 0.8 collective-permute-done.19
  111.7 2.2 %collective-permute-done.20 = bf16[32,2048]{1,0:T(8,128)(2,1)S(1)} collective-permute-done((bf16[32,2048]{1,0:T(8,128)(2,1)S(1)}, bf16[32,2048]{1,0:T(8,128)(2,1)S(1)}, u32[]{:S(2)}, u32[]{:S(2)}) %collective-permute-start.20) | collective-permute-done | bytes 131104 | tf_op jit(solution)/shard_map/ppermute | solution.py:32
  114.0 0.4 collective-permute-start.26
  114.5 4.7 %collective-permute-start.22 = (bf16[128,2048]{1,0:T(8,128)(2,1)S(1)}, bf16[128,2048]{1,0:T(8,128)(2,1)S(1)}, u32[]{:S(2)}, u32[]{:S(2)}) collective-permute-start(bf16[128,2048]{1,0:T(8,128)(2,1)S(1)} %pad_maximum_fusion), channel_id=1, source_target_pairs={{0,1},{1,0},{2,3},{3,2},{4,5},{5,4},{6,7},{7,6},{8,9},{9,8},{10,11... | collective-permute-start | bytes 1572872 | tf_op jit(solution)/shard_map/ppermute | solution.py:32
  119.2 1.5 collective-permute-done.22
  120.8 7.2 %collective-permute-done.25.low_far_ref = bf16[4,128,768]{2,1,0:T(8,128)(2,1)S(1)} collective-permute-done((bf16[4,128,768]{2,1,0:T(8,128)(2,1)S(1)}, bf16[4,128,768]{2,1,0:T(8,128)(2,1)S(1)}, u32[]{:S(2)}, u32[]{:S(2)}) %collective-permute-start.25) | collective-permute-done | bytes 786464 | tf_op jit(solution)/shard_map/ppermute | solution.py:32
  128.0 0.9 copy-done.7
  128.9 1.1 collective-permute-done.26.high_far_ref
  130.0 7.7 %feed_forward.1 = (f32[128,2048]{1,0:T(8,128)}, bf16[128,2048]{1,0:T(8,128)(2,1)}) custom-call(s32[10]{0:T(128)} %stack.43.place_ref, bf16[256,2048]{1,0:T(8,128)(2,1)} %copy-done.2, bf16[8,128,768]{2,1,0:T(8,128)(2,1)} %bitcast.20, bf16[4,128,768]{2,1,0:T(8,128)(2,1)} %copy-done.5, bf16[4,128,768]{2,1,0:T(8,128)(2,1)} %copy-done.4, ...), custom_call_target="tpu_custom_call" | custom-call | tf_op jit(solution)/shard_map/feed_forward/pallas_call | solution.py:369
  137.7 4.2 %collective-permute-start.27 = (bf16[128,2048]{1,0:T(8,128)(2,1)}, bf16[128,2048]{1,0:T(8,128)(2,1)S(1)}, u32[]{:S(2)}, u32[]{:S(2)}) collective-permute-start(bf16[128,2048]{1,0:T(8,128)(2,1)} %get-tuple-element.52), channel_id=1, source_target_pairs={{0,1},{1,0},{2,3},{3,2},{4,5},{5,4},{6,7},{7,6},{8,9},{9,8},{10,11... | collective-permute-start | bytes 1572872 | tf_op jit(solution)/shard_map/ppermute | solution.py:32
  141.9 1.7 %collective-permute-done.27 = bf16[128,2048]{1,0:T(8,128)(2,1)S(1)} collective-permute-done((bf16[128,2048]{1,0:T(8,128)(2,1)}, bf16[128,2048]{1,0:T(8,128)(2,1)S(1)}, u32[]{:S(2)}, u32[]{:S(2)}) %collective-permute-start.27) | collective-permute-done | bytes 524320 | tf_op jit(solution)/shard_map/ppermute | solution.py:32
  143.7 1.4 fusion.11
  145.1 0.8 collective-permute-start.28
  145.9 1.3 collective-permute-start.29
  147.1 0.8 collective-permute-start.30
  147.9 1.9 %collective-permute-done.28 = bf16[32,2048]{1,0:T(8,128)(2,1)S(1)} collective-permute-done((bf16[32,2048]{1,0:T(8,128)(2,1)S(1)}, bf16[32,2048]{1,0:T(8,128)(2,1)S(1)}, u32[]{:S(2)}, u32[]{:S(2)}) %collective-permute-start.28) | collective-permute-done | bytes 131104 | tf_op jit(solution)/shard_map/ppermute | solution.py:32
  149.8 2.0 %collective-permute-done.29 = bf16[32,2048]{1,0:T(8,128)(2,1)S(1)} collective-permute-done((bf16[32,2048]{1,0:T(8,128)(2,1)S(1)}, bf16[32,2048]{1,0:T(8,128)(2,1)S(1)}, u32[]{:S(2)}, u32[]{:S(2)}) %collective-permute-start.29) | collective-permute-done | bytes 131104 | tf_op jit(solution)/shard_map/ppermute | solution.py:32
  151.8 3.7 %collective-permute-done.30 = bf16[32,2048]{1,0:T(8,128)(2,1)S(1)} collective-permute-done((bf16[32,2048]{1,0:T(8,128)(2,1)S(1)}, bf16[32,2048]{1,0:T(8,128)(2,1)S(1)}, u32[]{:S(2)}, u32[]{:S(2)}) %collective-permute-start.30) | collective-permute-done | bytes 131104 | tf_op jit(solution)/shard_map/ppermute | solution.py:32
  155.4 0.7 fusion.6
  (69 shorter events, 0.5 us)
Async XLA Ops:
  6.5 51.5 %copy-start = (bf16[128,2048]{1,0:T(8,128)(2,1)S(1)}, bf16[128,2048]{1,0:T(8,128)(2,1)}, u32[]{:S(2)}) copy-start(bf16[128,2048]{1,0:T(8,128)(2,1)} %param.29) | copy-start | bytes 1572868
  6.5 43.9 %all-gather.5.cloned.1.call-start = ((), (), s32[]{:S(2)}) async-start(), calls=%async_computation | async-start | bytes 1769472 | tf_op jit(solution)/shard_map/all_gather | solution.py:423
  8.3 121.7 %all-gather.7.cloned.1.call-start = ((), (), s32[]{:S(2)}) async-start(), calls=%async_computation.1 | async-start | bytes 3538944 | tf_op jit(solution)/shard_map/all_gather | solution.py:451
  9.2 11.8 %collective-permute-start = (bf16[64,768]{1,0:T(8,128)(2,1)S(1)}, bf16[64,768]{1,0:T(8,128)(2,1)S(1)}, u32[]{:S(2)}, u32[]{:S(2)}) collective-permute-start(bf16[64,768]{1,0:T(8,128)(2,1)S(1)} %pad.8), channel_id=1, source_target_pairs={{0,8},{8,16},{16,24},{24,0},{1,9},{9,17},{17,25},{25,1},{2,10},{10... | collective-permute-start | bytes 294920 | tf_op jit(solution)/shard_map/ppermute | solution.py:32
  11.4 9.7 %collective-permute-start.1 = (bf16[64,768]{1,0:T(8,128)(2,1)S(1)}, bf16[64,768]{1,0:T(8,128)(2,1)S(1)}, u32[]{:S(2)}, u32[]{:S(2)}) collective-permute-start(bf16[64,768]{1,0:T(8,128)(2,1)S(1)} %pad.8), channel_id=1, source_target_pairs={{0,24},{8,0},{16,8},{24,16},{1,25},{9,1},{17,9},{25,17},{2,26},{10... | collective-permute-start | bytes 294920 | tf_op jit(solution)/shard_map/ppermute | solution.py:32
  13.0 8.1 %collective-permute-start.2 = (bf16[64,768]{1,0:T(8,128)(2,1)S(1)}, bf16[64,768]{1,0:T(8,128)(2,1)S(1)}, u32[]{:S(2)}, u32[]{:S(2)}) collective-permute-start(bf16[64,768]{1,0:T(8,128)(2,1)S(1)} %pad.8), channel_id=1, source_target_pairs={{0,16},{8,24},{16,0},{24,8},{1,17},{9,25},{17,1},{25,9},{2,18},{10... | collective-permute-start | bytes 294920 | tf_op jit(solution)/shard_map/ppermute | solution.py:32
  21.9 4.1 %collective-permute-start.3 = (f32[4,8,128]{2,1,0:T(8,128)}, f32[4,8,128]{2,1,0:T(8,128)S(1)}, u32[]{:S(2)}, u32[]{:S(2)}) collective-permute-start(f32[4,8,128]{2,1,0:T(8,128)} %get-tuple-element.30.own_ref), channel_id=1, source_target_pairs={{0,8},{8,16},{16,24},{24,0},{1,9},{9,17},{17,25},{25,1},{2,10},{10... | collective-permute-start | bytes 49160 | tf_op jit(solution)/shard_map/ppermute | solution.py:32
  22.4 3.6 %collective-permute-start.4 = (f32[4,8,128]{2,1,0:T(8,128)}, f32[4,8,128]{2,1,0:T(8,128)S(1)}, u32[]{:S(2)}, u32[]{:S(2)}) collective-permute-start(f32[4,8,128]{2,1,0:T(8,128)} %get-tuple-element.30.own_ref), channel_id=1, source_target_pairs={{0,24},{8,0},{16,8},{24,16},{1,25},{9,1},{17,9},{25,17},{2,26},{10... | collective-permute-start | bytes 49160 | tf_op jit(solution)/shard_map/ppermute | solution.py:32
  24.7 4.4 %collective-permute-start.5 = (f32[4,8,128]{2,1,0:T(8,128)}, f32[4,8,128]{2,1,0:T(8,128)S(1)}, u32[]{:S(2)}, u32[]{:S(2)}) collective-permute-start(f32[4,8,128]{2,1,0:T(8,128)} %get-tuple-element.30.own_ref), channel_id=1, source_target_pairs={{0,16},{8,24},{16,0},{24,8},{1,17},{9,25},{17,1},{25,9},{2,18},{10... | collective-permute-start | bytes 49160 | tf_op jit(solution)/shard_map/ppermute | solution.py:32
  26.0 3.0 %copy-start.9 = (f32[4,8,128]{2,1,0:T(8,128)}, f32[4,8,128]{2,1,0:T(8,128)S(1)}, u32[]{:S(2)}) copy-start(f32[4,8,128]{2,1,0:T(8,128)S(1)} %collective-permute-done.3.refs_0_) | copy-start | bytes 49156
  26.0 3.0 %copy-start.10 = (f32[4,8,128]{2,1,0:T(8,128)}, f32[4,8,128]{2,1,0:T(8,128)S(1)}, u32[]{:S(2)}) copy-start(f32[4,8,128]{2,1,0:T(8,128)S(1)} %collective-permute-done.4.refs_1_) | copy-start | bytes 49156
  29.0 0.6 copy-start.11
  31.1 10.2 %collective-permute-start.10 = (f32[4,8,128]{2,1,0:T(8,128)}, f32[4,8,128]{2,1,0:T(8,128)S(1)}, u32[]{:S(2)}, u32[]{:S(2)}) collective-permute-start(f32[4,8,128]{2,1,0:T(8,128)} %get-tuple-element.33.refs_0_), channel_id=1, source_target_pairs={{0,160},{32,192},{64,224},{96,0},{128,32},{160,64},{192,96},{224,1... | collective-permute-start | bytes 49160 | tf_op jit(solution)/shard_map/ppermute | solution.py:32
  37.5 6.0 %collective-permute-start.11 = (f32[4,8,128]{2,1,0:T(8,128)}, f32[4,8,128]{2,1,0:T(8,128)S(1)}, u32[]{:S(2)}, u32[]{:S(2)}) collective-permute-start(f32[4,8,128]{2,1,0:T(8,128)} %get-tuple-element.33.refs_0_), channel_id=1, source_target_pairs={{0,192},{32,224},{64,0},{96,32},{128,64},{160,96},{192,128},{224,1... | collective-permute-start | bytes 49160 | tf_op jit(solution)/shard_map/ppermute | solution.py:32
  37.8 8.5 %collective-permute-start.12 = (f32[4,8,128]{2,1,0:T(8,128)}, f32[4,8,128]{2,1,0:T(8,128)S(1)}, u32[]{:S(2)}, u32[]{:S(2)}) collective-permute-start(f32[4,8,128]{2,1,0:T(8,128)} %get-tuple-element.33.refs_0_), channel_id=1, source_target_pairs={{0,224},{32,0},{64,32},{96,64},{128,96},{160,128},{192,160},{224,1... | collective-permute-start | bytes 49160 | tf_op jit(solution)/shard_map/ppermute | solution.py:32
  38.2 8.0 %collective-permute-start.6 = (f32[4,8,128]{2,1,0:T(8,128)}, f32[4,8,128]{2,1,0:T(8,128)S(1)}, u32[]{:S(2)}, u32[]{:S(2)}) collective-permute-start(f32[4,8,128]{2,1,0:T(8,128)} %get-tuple-element.33.refs_0_), channel_id=1, source_target_pairs={{0,32},{32,64},{64,96},{96,128},{128,160},{160,192},{192,224},{224... | collective-permute-start | bytes 49160 | tf_op jit(solution)/shard_map/ppermute | solution.py:32
  39.4 6.9 %collective-permute-start.7 = (f32[4,8,128]{2,1,0:T(8,128)}, f32[4,8,128]{2,1,0:T(8,128)S(1)}, u32[]{:S(2)}, u32[]{:S(2)}) collective-permute-start(f32[4,8,128]{2,1,0:T(8,128)} %get-tuple-element.33.refs_0_), channel_id=1, source_target_pairs={{0,64},{32,96},{64,128},{96,160},{128,192},{160,224},{192,0},{224,... | collective-permute-start | bytes 49160 | tf_op jit(solution)/shard_map/ppermute | solution.py:32
  41.3 9.1 %copy-start.13 = (f32[4,8,128]{2,1,0:T(8,128)}, f32[4,8,128]{2,1,0:T(8,128)S(1)}, u32[]{:S(2)}) copy-start(f32[4,8,128]{2,1,0:T(8,128)S(1)} %collective-permute-done.10.refs_5_) | copy-start | bytes 49156
  41.3 5.8 %collective-permute-start.8 = (f32[4,8,128]{2,1,0:T(8,128)}, f32[4,8,128]{2,1,0:T(8,128)S(1)}, u32[]{:S(2)}, u32[]{:S(2)}) collective-permute-start(f32[4,8,128]{2,1,0:T(8,128)} %get-tuple-element.33.refs_0_), channel_id=1, source_target_pairs={{0,96},{32,128},{64,160},{96,192},{128,224},{160,0},{192,32},{224,... | collective-permute-start | bytes 49160 | tf_op jit(solution)/shard_map/ppermute | solution.py:32
  43.5 6.9 %copy-start.14 = (f32[4,8,128]{2,1,0:T(8,128)}, f32[4,8,128]{2,1,0:T(8,128)S(1)}, u32[]{:S(2)}) copy-start(f32[4,8,128]{2,1,0:T(8,128)S(1)} %collective-permute-done.11.refs_6_) | copy-start | bytes 49156
  43.5 6.9 %collective-permute-start.9 = (f32[4,8,128]{2,1,0:T(8,128)}, f32[4,8,128]{2,1,0:T(8,128)S(1)}, u32[]{:S(2)}, u32[]{:S(2)}) collective-permute-start(f32[4,8,128]{2,1,0:T(8,128)} %get-tuple-element.33.refs_0_), channel_id=1, source_target_pairs={{0,128},{32,160},{64,192},{96,224},{128,0},{160,32},{192,64},{224,... | collective-permute-start | bytes 49160 | tf_op jit(solution)/shard_map/ppermute | solution.py:32
  46.2 4.2 %copy-start.15 = (f32[4,8,128]{2,1,0:T(8,128)}, f32[4,8,128]{2,1,0:T(8,128)S(1)}, u32[]{:S(2)}) copy-start(f32[4,8,128]{2,1,0:T(8,128)S(1)} %collective-permute-done.12.refs_7_) | copy-start | bytes 49156
  46.3 4.2 %copy-start.16 = (f32[4,8,128]{2,1,0:T(8,128)}, f32[4,8,128]{2,1,0:T(8,128)S(1)}, u32[]{:S(2)}) copy-start(f32[4,8,128]{2,1,0:T(8,128)S(1)} %collective-permute-done.6.refs_1_) | copy-start | bytes 49156
  46.3 4.2 %copy-start.17 = (f32[4,8,128]{2,1,0:T(8,128)}, f32[4,8,128]{2,1,0:T(8,128)S(1)}, u32[]{:S(2)}) copy-start(f32[4,8,128]{2,1,0:T(8,128)S(1)} %collective-permute-done.7.refs_2_) | copy-start | bytes 49156
  47.1 3.3 %copy-start.18 = (f32[4,8,128]{2,1,0:T(8,128)}, f32[4,8,128]{2,1,0:T(8,128)S(1)}, u32[]{:S(2)}) copy-start(f32[4,8,128]{2,1,0:T(8,128)S(1)} %collective-permute-done.8.refs_3_) | copy-start | bytes 49156
  50.4 0.6 copy-start.19
  59.3 11.1 %copy-start.1 = (bf16[1024,768]{1,0:T(8,128)(2,1)S(1)}, bf16[1024,768]{1,0:T(8,128)(2,1)}, u32[]{:S(2)}) copy-start(bf16[1024,768]{1,0:T(8,128)(2,1)} %all-gather.5.cloned.1.call-done) | copy-start | bytes 4718596
  59.3 7.2 %collective-permute-start.13 = (bf16[128,2048]{1,0:T(8,128)(2,1)S(1)}, bf16[128,2048]{1,0:T(8,128)(2,1)S(1)}, u32[]{:S(2)}, u32[]{:S(2)}) collective-permute-start(bf16[128,2048]{1,0:T(8,128)(2,1)S(1)} %slice.79), channel_id=1, source_target_pairs={{0,1},{1,0},{2,3},{3,2},{4,5},{5,4},{6,7},{7,6},{8,9},{9,8},{10,11... | collective-permute-start | bytes 1572872 | tf_op jit(solution)/shard_map/ppermute | solution.py:32
  66.7 12.4 %copy-start.8 = (bf16[32,2048]{1,0:T(8,128)(2,1)S(1)}, bf16[32,2048]{1,0:T(8,128)(2,1)}, u32[]{:S(2)}) copy-start(bf16[32,2048]{1,0:T(8,128)(2,1)} %param.18) | copy-start | bytes 393220
  66.7 7.7 %collective-permute-start.14 = (bf16[32,2048]{1,0:T(8,128)(2,1)S(1)}, bf16[32,2048]{1,0:T(8,128)(2,1)S(1)}, u32[]{:S(2)}, u32[]{:S(2)}) collective-permute-start(bf16[32,2048]{1,0:T(8,128)(2,1)S(1)} %get-tuple-element.64), channel_id=1, source_target_pairs={{0,6},{2,0},{4,2},{6,4},{1,7},{3,1},{5,3},{7,5},{8,14},{10,8},{12,... | collective-permute-start | bytes 393224 | tf_op jit(solution)/shard_map/ppermute | solution.py:32
  69.3 5.9 %collective-permute-start.15 = (bf16[32,2048]{1,0:T(8,128)(2,1)S(1)}, bf16[32,2048]{1,0:T(8,128)(2,1)S(1)}, u32[]{:S(2)}, u32[]{:S(2)}) collective-permute-start(bf16[32,2048]{1,0:T(8,128)(2,1)S(1)} %get-tuple-element.66), channel_id=1, source_target_pairs={{0,4},{2,6},{4,0},{6,2},{1,5},{3,7},{5,1},{7,3},{8,12},{10,14},{12... | collective-permute-start | bytes 393224 | tf_op jit(solution)/shard_map/ppermute | solution.py:32
  69.8 9.5 %copy-start.12 = (f32[2048]{0:T(1024)S(1)}, f32[2048]{0:T(1024)}, u32[]{:S(2)}) copy-start(f32[2048]{0:T(1024)} %param.30) | copy-start | bytes 24580
  69.8 9.3 %collective-permute-start.16 = (bf16[32,2048]{1,0:T(8,128)(2,1)S(1)}, bf16[32,2048]{1,0:T(8,128)(2,1)S(1)}, u32[]{:S(2)}, u32[]{:S(2)}) collective-permute-start(bf16[32,2048]{1,0:T(8,128)(2,1)S(1)} %get-tuple-element.65), channel_id=1, source_target_pairs={{0,2},{2,4},{4,6},{6,0},{1,3},{3,5},{5,7},{7,1},{8,10},{10,12},{12... | collective-permute-start | bytes 393224 | tf_op jit(solution)/shard_map/ppermute | solution.py:32
  70.5 36.1 %collective-permute-start.18 = (bf16[4,128,768]{2,1,0:T(8,128)(2,1)S(1)}, bf16[4,128,768]{2,1,0:T(8,128)(2,1)S(1)}, u32[]{:S(2)}, u32[]{:S(2)}) collective-permute-start(bf16[4,128,768]{2,1,0:T(8,128)(2,1)S(1)} %get-tuple-element.59), channel_id=1, source_target_pairs={{0,24},{8,0},{16,8},{24,16},{1,25},{9,1},{17,9},{25,17},{2,26},{10... | collective-permute-start | bytes 2359304 | tf_op jit(solution)/shard_map/ppermute | solution.py:32
  70.6 50.2 %collective-permute-start.23 = (bf16[4,128,768]{2,1,0:T(8,128)(2,1)S(1)}, bf16[4,128,768]{2,1,0:T(8,128)(2,1)S(1)}, u32[]{:S(2)}, u32[]{:S(2)}) collective-permute-start(bf16[4,128,768]{2,1,0:T(8,128)(2,1)S(1)} %get-tuple-element.59), channel_id=1, source_target_pairs={{0,8},{8,16},{16,24},{24,0},{1,9},{9,17},{17,25},{25,1},{2,10},{10... | collective-permute-start | bytes 2359304 | tf_op jit(solution)/shard_map/ppermute | solution.py:32
  74.4 32.2 %collective-permute-start.17 = (bf16[4,128,768]{2,1,0:T(8,128)(2,1)S(1)}, bf16[4,128,768]{2,1,0:T(8,128)(2,1)S(1)}, u32[]{:S(2)}, u32[]{:S(2)}) collective-permute-start(bf16[4,128,768]{2,1,0:T(8,128)(2,1)S(1)} %get-tuple-element.60), channel_id=1, source_target_pairs={{0,8},{8,16},{16,24},{24,0},{1,9},{9,17},{17,25},{25,1},{2,10},{10... | collective-permute-start | bytes 2359304 | tf_op jit(solution)/shard_map/ppermute | solution.py:32
  75.2 45.6 %collective-permute-start.24 = (bf16[4,128,768]{2,1,0:T(8,128)(2,1)S(1)}, bf16[4,128,768]{2,1,0:T(8,128)(2,1)S(1)}, u32[]{:S(2)}, u32[]{:S(2)}) collective-permute-start(bf16[4,128,768]{2,1,0:T(8,128)(2,1)S(1)} %get-tuple-element.60), channel_id=1, source_target_pairs={{0,24},{8,0},{16,8},{24,16},{1,25},{9,1},{17,9},{25,17},{2,26},{10... | collective-permute-start | bytes 2359304 | tf_op jit(solution)/shard_map/ppermute | solution.py:32
  106.6 14.2 %copy-start.5 = (bf16[4,128,768]{2,1,0:T(8,128)(2,1)}, bf16[4,128,768]{2,1,0:T(8,128)(2,1)S(1)}, u32[]{:S(2)}) copy-start(bf16[4,128,768]{2,1,0:T(8,128)(2,1)S(1)} %collective-permute-done.17.low_left_ref) | copy-start | bytes 2359300
  106.6 23.3 %copy-start.3 = (bf16[4,128,768]{2,1,0:T(8,128)(2,1)}, bf16[4,128,768]{2,1,0:T(8,128)(2,1)S(1)}, u32[]{:S(2)}) copy-start(bf16[4,128,768]{2,1,0:T(8,128)(2,1)S(1)} %collective-permute-done.18.high_right_ref) | copy-start | bytes 2359300
  106.6 5.1 %collective-permute-start.19 = (bf16[32,2048]{1,0:T(8,128)(2,1)S(1)}, bf16[32,2048]{1,0:T(8,128)(2,1)S(1)}, u32[]{:S(2)}, u32[]{:S(2)}) collective-permute-start(bf16[32,2048]{1,0:T(8,128)(2,1)S(1)} %multiply_convert_fusion), channel_id=1, source_target_pairs={{0,2},{2,4},{4,6},{6,0},{1,3},{3,5},{5,7},{7,1},{8,10},{10,12},{12... | collective-permute-start | bytes 393224 | tf_op jit(solution)/shard_map/ppermute | solution.py:32
  108.2 5.8 %collective-permute-start.20 = (bf16[32,2048]{1,0:T(8,128)(2,1)S(1)}, bf16[32,2048]{1,0:T(8,128)(2,1)S(1)}, u32[]{:S(2)}, u32[]{:S(2)}) collective-permute-start(bf16[32,2048]{1,0:T(8,128)(2,1)S(1)} %multiply_convert_fusion), channel_id=1, source_target_pairs={{0,4},{2,6},{4,0},{6,2},{1,5},{3,7},{5,1},{7,3},{8,12},{10,14},{12... | collective-permute-start | bytes 393224 | tf_op jit(solution)/shard_map/ppermute | solution.py:32
  110.0 4.5 %collective-permute-start.21 = (bf16[32,2048]{1,0:T(8,128)(2,1)S(1)}, bf16[32,2048]{1,0:T(8,128)(2,1)S(1)}, u32[]{:S(2)}, u32[]{:S(2)}) collective-permute-start(bf16[32,2048]{1,0:T(8,128)(2,1)S(1)} %multiply_convert_fusion), channel_id=1, source_target_pairs={{0,6},{2,0},{4,2},{6,4},{1,7},{3,1},{5,3},{7,5},{8,14},{10,8},{12,... | collective-permute-start | bytes 393224 | tf_op jit(solution)/shard_map/ppermute | solution.py:32
  111.7 16.2 %collective-permute-start.25 = (bf16[4,128,768]{2,1,0:T(8,128)(2,1)S(1)}, bf16[4,128,768]{2,1,0:T(8,128)(2,1)S(1)}, u32[]{:S(2)}, u32[]{:S(2)}) collective-permute-start(bf16[4,128,768]{2,1,0:T(8,128)(2,1)S(1)} %collective-permute-done.17.low_left_ref), channel_id=1, source_target_pairs={{0,8},{8,16},{16,24},{24,0},{1,9},{9,17},{17,25},{25,1},{2,10},{10... | collective-permute-start | bytes 2359304 | tf_op jit(solution)/shard_map/ppermute | solution.py:32
  114.0 16.0 %collective-permute-start.26 = (bf16[4,128,768]{2,1,0:T(8,128)(2,1)S(1)}, bf16[4,128,768]{2,1,0:T(8,128)(2,1)}, u32[]{:S(2)}, u32[]{:S(2)}) collective-permute-start(bf16[4,128,768]{2,1,0:T(8,128)(2,1)S(1)} %collective-permute-done.18.high_right_ref), channel_id=1, source_target_pairs={{0,24},{8,0},{16,8},{24,16},{1,25},{9,1},{17,9},{25,17},{2,26},{10... | collective-permute-start | bytes 2359304 | tf_op jit(solution)/shard_map/ppermute | solution.py:32
  114.5 6.3 %collective-permute-start.22 = (bf16[128,2048]{1,0:T(8,128)(2,1)S(1)}, bf16[128,2048]{1,0:T(8,128)(2,1)S(1)}, u32[]{:S(2)}, u32[]{:S(2)}) collective-permute-start(bf16[128,2048]{1,0:T(8,128)(2,1)S(1)} %pad_maximum_fusion), channel_id=1, source_target_pairs={{0,1},{1,0},{2,3},{3,2},{4,5},{5,4},{6,7},{7,6},{8,9},{9,8},{10,11... | collective-permute-start | bytes 1572872 | tf_op jit(solution)/shard_map/ppermute | solution.py:32
  120.8 9.2 %copy-start.2 = (bf16[256,2048]{1,0:T(8,128)(2,1)}, bf16[256,2048]{1,0:T(8,128)(2,1)S(1)}, u32[]{:S(2)}) copy-start(bf16[256,2048]{1,0:T(8,128)(2,1)S(1)} %constant_dynamic-update-slice_fusion.rows_ref) | copy-start | bytes 3145732
  120.8 9.2 %copy-start.4 = (bf16[4,128,768]{2,1,0:T(8,128)(2,1)}, bf16[4,128,768]{2,1,0:T(8,128)(2,1)S(1)}, u32[]{:S(2)}) copy-start(bf16[4,128,768]{2,1,0:T(8,128)(2,1)S(1)} %collective-permute-done.23.high_left_ref) | copy-start | bytes 2359300
  120.8 7.2 %copy-start.6 = (bf16[4,128,768]{2,1,0:T(8,128)(2,1)}, bf16[4,128,768]{2,1,0:T(8,128)(2,1)S(1)}, u32[]{:S(2)}) copy-start(bf16[4,128,768]{2,1,0:T(8,128)(2,1)S(1)} %collective-permute-done.24.low_right_ref) | copy-start | bytes 2359300
  128.0 0.9 copy-start.7
  137.7 5.9 %collective-permute-start.27 = (bf16[128,2048]{1,0:T(8,128)(2,1)}, bf16[128,2048]{1,0:T(8,128)(2,1)S(1)}, u32[]{:S(2)}, u32[]{:S(2)}) collective-permute-start(bf16[128,2048]{1,0:T(8,128)(2,1)} %get-tuple-element.52), channel_id=1, source_target_pairs={{0,1},{1,0},{2,3},{3,2},{4,5},{5,4},{6,7},{7,6},{8,9},{9,8},{10,11... | collective-permute-start | bytes 1572872 | tf_op jit(solution)/shard_map/ppermute | solution.py:32
  145.1 4.8 %collective-permute-start.28 = (bf16[32,2048]{1,0:T(8,128)(2,1)S(1)}, bf16[32,2048]{1,0:T(8,128)(2,1)S(1)}, u32[]{:S(2)}, u32[]{:S(2)}) collective-permute-start(bf16[32,2048]{1,0:T(8,128)(2,1)S(1)} %get-tuple-element.61), channel_id=1, source_target_pairs={{0,6},{2,0},{4,2},{6,4},{1,7},{3,1},{5,3},{7,5},{8,14},{10,8},{12,... | collective-permute-start | bytes 393224 | tf_op jit(solution)/shard_map/ppermute | solution.py:32
  145.9 5.9 %collective-permute-start.29 = (bf16[32,2048]{1,0:T(8,128)(2,1)S(1)}, bf16[32,2048]{1,0:T(8,128)(2,1)S(1)}, u32[]{:S(2)}, u32[]{:S(2)}) collective-permute-start(bf16[32,2048]{1,0:T(8,128)(2,1)S(1)} %get-tuple-element.63), channel_id=1, source_target_pairs={{0,4},{2,6},{4,0},{6,2},{1,5},{3,7},{5,1},{7,3},{8,12},{10,14},{12... | collective-permute-start | bytes 393224 | tf_op jit(solution)/shard_map/ppermute | solution.py:32
  147.1 8.3 %collective-permute-start.30 = (bf16[32,2048]{1,0:T(8,128)(2,1)S(1)}, bf16[32,2048]{1,0:T(8,128)(2,1)S(1)}, u32[]{:S(2)}, u32[]{:S(2)}) collective-permute-start(bf16[32,2048]{1,0:T(8,128)(2,1)S(1)} %get-tuple-element.62), channel_id=1, source_target_pairs={{0,2},{2,4},{4,6},{6,0},{1,3},{3,5},{5,7},{7,1},{8,10},{10,12},{12... | collective-permute-start | bytes 393224 | tf_op jit(solution)/shard_map/ppermute | solution.py:32
Sparse Core Ops, SparseCore 0:
  9.1 39.9 all-gather.4
  50.9 46.9 all-gather.6
